TPU v7x, 256 devices: a whole 4x4x8 slice. The times are simulated.
256 devices in a mesh: sp: 64 (over z, x, core), tp: 4 (over y).
Axes of the slice: x: 4, y: 4, z: 8, core: 2. Of those that a mesh axis runs over, the one named last changes fastest.
Arguments:
- tokens: bfloat16 [8192, 2048], P('sp'), may hold values from -6 to 6
- norm_gain: float32 [2048], replicated, may hold values from 0.1 to 1.9
- cotangent: bfloat16 [8192, 2048], P('sp'), may hold values from -16 to 16
- routes: int32 [8192, 2], P('sp'), may hold values from 0 to 31, all different within a row; in each aligned block of 128 rows (0 to 127, 128 to 255, ...) at most 16 rows name the same one
- route_weight: float32 [8192, 2], P('sp'), may hold values from 0.2 to 1
- gate_weight: bfloat16 [64, 2048, 1792], P('sp', None, 'tp'), may hold values from -0.125 to 0.125
- up_weight: bfloat16 [64, 2048, 1792], P('sp', None, 'tp'), may hold values from -0.125 to 0.125
- down_weight: bfloat16 [64, 1792, 2048], P('sp', 'tp'), may hold values from -0.09375 to 0.09375
- scan_input: bfloat16 [8192, 1024], P('sp', 'tp'), may hold values from -6 to 6
- out_gate: bfloat16 [8192, 1024], P('sp', 'tp'), may hold values from -6 to 6
- step_size: float32 [16, 8192], P('tp', 'sp'), may hold values from 0.24 to 4.1
- decay_rate: float32 [16], P('tp'), may hold values from 1.2084961e-06 to 0.031
- write_keys: bfloat16 [8192, 256], P('sp', 'tp'), may hold values from -0.75 to 0.75
- read_keys: bfloat16 [8192, 256], P('sp', 'tp'), may hold values from -0.75 to 0.75
- start_state: float32 [64, 16, 64, 64], P('sp', 'tp'), may hold values from -12 to 12
- out_proj: bfloat16 [2048, 1024], P(None, 'tp'), may hold values from -0.1875 to 0.1875
Outputs:
- residual_grad: bfloat16 [8192, 2048], P('sp', 'tp')
- gate_weight_grad: bfloat16 [64, 2048, 1792], P('sp', None, 'tp')
- up_weight_grad: bfloat16 [64, 2048, 1792], P('sp', None, 'tp')
- down_weight_grad: bfloat16 [64, 1792, 2048], P('sp', 'tp')
- out_proj_grad: float32 [2048, 1024], P('sp', 'tp')
- scan_input_grad: bfloat16 [8192, 1024], P('sp', 'tp')
- out_gate_grad: bfloat16 [8192, 1024], P('sp', 'tp')
- write_keys_grad: bfloat16 [8192, 256], P('sp', 'tp')
- read_keys_grad: bfloat16 [8192, 256], P('sp', 'tp')
Inputs may be any that keep to these rules, and one draw needn't show every extreme that they name: Each token names two different experts. Among the tokens of one block of 128 positions at most 16 routes name one expert, and in every draw some expert gets exactly 16 routes from some block.
All inputs are finite; a program needn't handle non-finite values.
Results may differ from a plain program's by a relative error of at most 0.0078.
Values may be sent and summed in bfloat16 or wider, within the bound.
A program may use at most 128 MiB of HBM per device.

v0:
```python
import jax
import jax.numpy as jnp
from jax import lax
from jax.sharding import Mesh
from jax.sharding import PartitionSpec as P

D = 2048
HEADS = 16
STATE = 64
GROUPS = 4
SP = ("sp_0", "sp_1", "sp_2")


EPS = 1e-06
HIGHEST = lax.Precision.HIGHEST


def side_by_side(arrays, axis, split_dim, concat_dim, along):
    both = jnp.concatenate(arrays, axis=along)
    filled, at, finished = (
        lax.all_to_all(both, axis, split_axis=split_dim, concat_axis=concat_dim, tiled=True),
        0,
        [],
    )
    for a in arrays:
        finished.append(lax.slice_in_dim(filled, at, at + a.shape[along], axis=along))
        at += a.shape[along]
    return tuple(finished)


def swapped(value, axis, apart):
    mask = 2**apart
    pairs = [(source, source ^ mask) for source in range(lax.axis_size(axis))]
    return lax.ppermute(value, axis, pairs)


def joined_along(blocks, dim):
    lengths = list(blocks.shape[1:])
    lengths[dim] *= blocks.shape[0]
    return jnp.moveaxis(blocks, 0, dim).reshape(lengths)


def sent_to_all(array, axis):
    peers = lax.axis_size(axis)
    return lax.all_to_all(
        jnp.broadcast_to(array[None], (peers, *array.shape)), axis, 0, 0, tiled=True
    )


def gathered_copies(array, axis, dim):
    return joined_along(sent_to_all(array, axis), dim)


def filled_with(array, identity):
    return jax.tree.map(
        lambda a, e: jnp.broadcast_to(jnp.asarray(e, a.dtype), a.shape), array, identity
    )


def all_in_one(array, axis):
    leaves = jax.tree.leaves(array)
    sequence = sorted(range(len(leaves)), key=lambda k: -leaves[k].size)
    width = (1, *leaves[sequence[0]].shape)[-1]
    lines = [
        jnp.pad(leaves[k].reshape(-1), (0, -leaves[k].size % width)).reshape(-1, width)
        for k in sequence
    ]
    both, at, found = (lax.all_gather(jnp.concatenate(lines), axis), 0, {})
    for k, line in zip(sequence, lines):
        section = both[:, at : at + len(line)].reshape(len(both), -1)
        found[k] = section[:, : leaves[k].size].reshape(-1, *leaves[k].shape)
        at += len(line)
    numbers = iter(range(len(leaves)))
    return jax.tree.map(lambda _: found[next(numbers)], array)


def entering(array, axes, combine, identity):
    before = start = filled_with(array, identity)
    total = array
    for axis in reversed(axes):
        peers, index = (lax.axis_size(axis), lax.axis_index(axis))
        pieces = all_in_one(total, axis)
        inside, total = (start, start)
        for k in reversed(range(peers)):
            passed = k > index
            total = combine(total, jax.tree.map(lambda part: part[k], pieces))
            inside = jax.tree.map(lambda new, old: jnp.where(passed, new, old), total, inside)
        before = combine(inside, before)
    return before


def in_blocks(array, dim, peers):
    lengths = array.shape
    blocks = array.reshape(*lengths[:dim], peers, lengths[dim] // peers, *lengths[dim + 1 :])
    return jnp.moveaxis(blocks, dim, 0)


def summed_on_arrival(array, axis, dim):
    blocks = in_blocks(array, dim, lax.axis_size(axis))
    arrived = lax.all_to_all(blocks, axis, split_axis=0, concat_axis=0, tiled=True)
    return arrived.sum(axis=0)


def prepare(scan_rows, step_rows, write_rows, read_rows, decay_rates, per_group):
    length = scan_rows.shape[0]
    head_count = step_rows.shape[0]
    logdec = jnp.cumsum(-decay_rates[:, None] * step_rows, axis=1)
    causal = jnp.arange(length)[:, None] >= jnp.arange(length)[None, :]
    spread = jnp.where(causal[None, :, :], logdec[:, :, None] - logdec[:, None, :], -jnp.inf)
    weights = jnp.exp(spread)
    inputs = (
        scan_rows.astype(jnp.float32).reshape(length, head_count, -1)
        * jnp.transpose(step_rows)[:, :, None]
    )
    write_head = jnp.repeat(
        write_rows.astype(jnp.float32).reshape(length, -1, STATE), per_group, axis=1
    )
    read_head = jnp.repeat(
        read_rows.astype(jnp.float32).reshape(length, -1, STATE), per_group, axis=1
    )
    scores = jnp.einsum("thn,shn->hts", read_head, write_head, precision=HIGHEST) * weights
    return (logdec, weights, inputs, write_head, read_head, scores)


def block_forward(
    scan_rows,
    gate_rows,
    step_rows,
    write_rows,
    read_rows,
    decay_rates,
    entry_state,
    mix_grad,
    per_group,
):
    logdec, weights, inputs, write_head, read_head, scores = prepare(
        scan_rows, step_rows, write_rows, read_rows, decay_rates, per_group
    )
    length, head_count = (inputs.shape[0], inputs.shape[1])
    growth = jnp.transpose(jnp.exp(logdec))
    output = jnp.einsum("hts,shp->thp", scores, inputs, precision=HIGHEST)
    output = output + growth[:, :, None] * jnp.einsum(
        "thn,hpn->thp", read_head, entry_state, precision=HIGHEST
    )
    gate_val = gate_rows.astype(jnp.float32).reshape(length, head_count, -1)
    sigmoid_val = jax.nn.sigmoid(gate_val)
    gated = (output * gate_val * sigmoid_val).reshape(length, -1).astype(jnp.bfloat16)
    out_grad = mix_grad.reshape(length, head_count, -1)
    state_grad = out_grad * gate_val * sigmoid_val
    gate_grad = (
        (out_grad * output * sigmoid_val * (1.0 + gate_val * (1.0 - sigmoid_val)))
        .reshape(length, -1)
        .astype(jnp.bfloat16)
    )
    carried = jnp.einsum("th,thp,thn->hpn", growth, state_grad, read_head, precision=HIGHEST)
    return (gated, gate_grad, jnp.exp(logdec[:, -1]), carried, state_grad)


def block_back(
    scan_rows,
    step_rows,
    write_rows,
    read_rows,
    decay_rates,
    entry_state,
    state_grad,
    later_state,
    per_group,
):
    logdec, weights, inputs, write_head, read_head, scores = prepare(
        scan_rows, step_rows, write_rows, read_rows, decay_rates, per_group
    )
    length, head_count = (inputs.shape[0], inputs.shape[1])
    growth = jnp.transpose(jnp.exp(logdec))
    shrink = jnp.transpose(jnp.exp(logdec[:, -1:] - logdec))
    in_grad = jnp.einsum("hts,thp->shp", scores, state_grad, precision=HIGHEST)
    in_grad = in_grad + shrink[:, :, None] * jnp.einsum(
        "shn,hpn->shp", write_head, later_state, precision=HIGHEST
    )
    scan_grad = (
        (in_grad * jnp.transpose(step_rows)[:, :, None]).reshape(length, -1).astype(jnp.bfloat16)
    )
    pair_terms = jnp.einsum("thp,shp->hts", state_grad, inputs, precision=HIGHEST) * weights
    read_grad = jnp.einsum("hts,shn->thn", pair_terms, write_head, precision=HIGHEST)
    read_grad = read_grad + growth[:, :, None] * jnp.einsum(
        "thp,hpn->thn", state_grad, entry_state, precision=HIGHEST
    )
    write_grad = jnp.einsum("hts,thn->shn", pair_terms, read_head, precision=HIGHEST)
    write_grad = write_grad + shrink[:, :, None] * jnp.einsum(
        "shp,hpn->shn", inputs, later_state, precision=HIGHEST
    )
    group_count = head_count // per_group
    read_total = (
        jnp.sum(read_grad.reshape(length, group_count, per_group, -1), axis=2)
        .reshape(length, -1)
        .astype(jnp.bfloat16)
    )
    write_total = (
        jnp.sum(write_grad.reshape(length, group_count, per_group, -1), axis=2)
        .reshape(length, -1)
        .astype(jnp.bfloat16)
    )
    return (scan_grad, write_total, read_total)


def expert_grads(rows_in, rows_cot, gate_mat, up_mat, down_mat):
    contract_rows = (((0,), (0,)), ((), ()))
    contract_cols = (((1,), (1,)), ((), ()))
    gate_pre = jnp.dot(rows_in, gate_mat, preferred_element_type=jnp.float32)
    up_pre = jnp.dot(rows_in, up_mat, preferred_element_type=jnp.float32)
    sigmoid_val = jax.nn.sigmoid(gate_pre)
    active = (gate_pre * sigmoid_val * up_pre).astype(jnp.bfloat16)
    down_grad = lax.dot_general(active, rows_cot, contract_rows, preferred_element_type=jnp.float32)
    act_grad = lax.dot_general(
        rows_cot, down_mat, contract_cols, preferred_element_type=jnp.float32
    )
    gate_pre_grad = (
        act_grad * up_pre * sigmoid_val * (1.0 + gate_pre * (1.0 - sigmoid_val))
    ).astype(jnp.bfloat16)
    up_pre_grad = (act_grad * gate_pre * sigmoid_val).astype(jnp.bfloat16)
    gate_grad = lax.dot_general(
        rows_in, gate_pre_grad, contract_rows, preferred_element_type=jnp.float32
    )
    up_grad = lax.dot_general(
        rows_in, up_pre_grad, contract_rows, preferred_element_type=jnp.float32
    )
    input_grad = lax.dot_general(
        gate_pre_grad, gate_mat, contract_cols, preferred_element_type=jnp.float32
    )
    input_grad = input_grad + lax.dot_general(
        up_pre_grad, up_mat, contract_cols, preferred_element_type=jnp.float32
    )
    return (gate_grad, up_grad, down_grad, input_grad)


def compose(higher, nearer):
    return (nearer[0] * higher[0], nearer[1] + nearer[0][:, None, None] * higher[1])


def shards(
    tokens,
    norm_gain,
    cotangent,
    routes,
    route_weight,
    gate_weight,
    up_weight,
    down_weight,
    scan_input,
    out_gate,
    step_size,
    decay_rate,
    write_keys,
    read_keys,
    start_state,
    out_proj,
):
    sp_count = lax.axis_size(SP)
    tp_count = lax.axis_size("tp")
    tok_rows = tokens.shape[0]
    experts_count = sp_count // 2
    capacity = min(tok_rows, 4 * tok_rows // experts_count)
    quarter = D // tp_count
    hidden = tokens.astype(jnp.float32)
    inverse = lax.rsqrt(jnp.mean(hidden * hidden, axis=1) + EPS)
    normed = (hidden * inverse[:, None] * norm_gain[None, :]).astype(jnp.bfloat16)
    route_flat = routes.reshape(-1)
    member = (route_flat[:, None] == jnp.arange(experts_count, dtype=jnp.int32)[None, :]).astype(
        jnp.int32
    )
    earlier_count = jnp.sum((jnp.cumsum(member, axis=0) - member) * member, axis=1)
    places = (route_flat * capacity + earlier_count).reshape(tok_rows, 2)
    slot_ids = jnp.arange(experts_count * capacity, dtype=jnp.int32)[:, None]
    first_hit = slot_ids == places[None, :, 0]
    second_hit = slot_ids == places[None, :, 1]
    placing = jnp.logical_or(first_hit, second_hit)
    place_matrix = placing.astype(jnp.bfloat16)
    slot_weight = jnp.sum(
        jnp.where(first_hit, route_weight[None, :, 0], 0.0)
        + jnp.where(second_hit, route_weight[None, :, 1], 0.0),
        axis=1,
    )
    send_in = jnp.dot(place_matrix, normed, preferred_element_type=jnp.float32).astype(jnp.bfloat16)
    send_cot = (
        slot_weight[:, None] * jnp.dot(place_matrix, cotangent, preferred_element_type=jnp.float32)
    ).astype(jnp.bfloat16)
    half_cap = capacity // 2
    part_in, part_cot = side_by_side(
        (send_in.reshape(sp_count, half_cap, D), send_cot.reshape(sp_count, half_cap, D)),
        SP,
        0,
        0,
        1,
    )
    other_in, other_cot = swapped((part_in, part_cot), SP, 0)
    lower_bit = lax.axis_index(SP) % 2 == 0
    recv_in = jnp.concatenate(
        [jnp.where(lower_bit, part_in, other_in), jnp.where(lower_bit, other_in, part_in)], axis=1
    )
    recv_cot = jnp.concatenate(
        [jnp.where(lower_bit, part_cot, other_cot), jnp.where(lower_bit, other_cot, part_cot)],
        axis=1,
    )
    rows_in = recv_in.reshape(-1, D)
    rows_cot = recv_cot.reshape(-1, D)
    gate_grad, up_grad, down_grad, input_part = expert_grads(
        rows_in, rows_cot, gate_weight[0], up_weight[0], down_weight[0]
    )
    input_quarter = lax.psum_scatter(input_part, "tp", scatter_dimension=1, tiled=True)
    returned = lax.all_to_all(
        input_quarter.reshape(sp_count, capacity, quarter).astype(jnp.bfloat16),
        SP,
        split_axis=0,
        concat_axis=0,
        tiled=True,
    ).astype(jnp.float32)
    pair_total = jnp.sum(returned.reshape(experts_count, 2, capacity, quarter), axis=1).reshape(
        -1, quarter
    )
    token_quarter = lax.dot_general(
        placing.astype(jnp.float32), pair_total, (((0,), (0,)), ((), ())), precision=HIGHEST
    )
    normed_grad = gathered_copies(token_quarter, "tp", 1)
    gained = norm_gain[None, :] * normed_grad
    dotted = jnp.sum(hidden * gained, axis=1)
    residual = (
        cotangent.astype(jnp.float32)
        + inverse[:, None] * gained
        - hidden * (inverse**3 * dotted / D)[:, None]
    )
    residual_grad = residual.astype(jnp.bfloat16)
    mix_grad = jnp.dot(residual_grad, out_proj, preferred_element_type=jnp.float32)
    per_group = HEADS // GROUPS
    gated, gate_out_grad, decay_now, carried, state_grad = block_forward(
        scan_input,
        out_gate,
        step_size,
        write_keys,
        read_keys,
        decay_rate,
        start_state[0],
        mix_grad,
        per_group,
    )
    totals, later_state = entering(
        (decay_now, carried), SP, compose, (jnp.ones_like(decay_now), jnp.zeros_like(carried))
    )
    scan_grad, write_grad, read_grad = block_back(
        scan_input,
        step_size,
        write_keys,
        read_keys,
        decay_rate,
        start_state[0],
        state_grad,
        later_state,
        per_group,
    )
    out_proj_grad = summed_on_arrival(
        lax.dot_general(
            residual_grad, gated, (((0,), (0,)), ((), ())), preferred_element_type=jnp.float32
        ),
        SP,
        0,
    )
    residual_part = lax.dynamic_slice_in_dim(
        residual_grad, lax.axis_index("tp") * quarter, quarter, 1
    )
    return (
        residual_part,
        gate_grad.astype(jnp.bfloat16)[None],
        up_grad.astype(jnp.bfloat16)[None],
        down_grad.astype(jnp.bfloat16)[None],
        out_proj_grad,
        scan_grad,
        gate_out_grad,
        write_grad,
        read_grad,
    )


def solution(mesh):
    finer = Mesh(mesh.devices.reshape(8, 4, 2, mesh.shape["tp"]), ("sp_0", "sp_1", "sp_2", "tp"))
    in_specs = (
        P(SP, None),
        P(),
        P(SP, None),
        P(SP, None),
        P(SP, None),
        P(SP, None, "tp"),
        P(SP, None, "tp"),
        P(SP, "tp", None),
        P(SP, "tp"),
        P(SP, "tp"),
        P("tp", SP),
        P("tp"),
        P(SP, "tp"),
        P(SP, "tp"),
        P(SP, "tp", None, None),
        P(None, "tp"),
    )
    out_specs = (
        P(SP, "tp"),
        P(SP, None, "tp"),
        P(SP, None, "tp"),
        P(SP, "tp", None),
        P(SP, "tp"),
        P(SP, "tp"),
        P(SP, "tp"),
        P(SP, "tp"),
        P(SP, "tp"),
    )
    return jax.shard_map(
        shards, mesh=finer, in_specs=in_specs, out_specs=out_specs, check_vma=False
    )
```

profile of v0, /device:TPU:1, one launch (start us, length us, event | category | flops | bytes accessed | tf_op | source)
XLA Modules:
  0.0 393.6 jit_solution(8729033673943875722)
XLA Ops:
  11.1 1.3 copy.191
  15.5 107.4 %all_to_all.20 = bf16[64,16,2048]{2,1,0:T(8,128)(2,1)S(1)} all-to-all(bf16[64,16,2048]{2,1,0:T(8,128)(2,1)S(1)} %pad_maximum_fusion), channel_id=1, replica_groups=mesh['sp_0'=8,'sp_1'=4,'sp_2'=2,'tp'=4] {'sp_0','sp_1','sp_2'}, dimensions={0} | all-to-all | bytes 8388608 | tf_op jit(solution)/shard_map/all_to_all | solution.py:21
  123.0 1.6 slice.210
  125.6 2.1 collective-permute-start
  127.6 4.1 %collective-permute-done = bf16[64,8,2048]{2,1,0:T(8,128)(2,1)} collective-permute-done((bf16[64,8,2048]{2,1,0:T(8,128)(2,1)}, bf16[64,8,2048]{2,1,0:T(8,128)(2,1)}, u32[]{:S(2)}, u32[]{:S(2)}) %collective-permute-start) | collective-permute-done | bytes 2097184 | tf_op jit(solution)/shard_map/ppermute | solution.py:34
  131.8 3.3 broadcast_select_fusion.3
  136.0 3.5 collective-permute-done.1
  140.4 2.1 fusion.7
  143.2 2.1 fusion.10
  145.4 2.6 multiply_convert_fusion.2
  148.1 2.4 fusion.5
  150.5 5.9 %convolution_add_fusion = f32[1024,2048]{1,0:T(8,128)} fusion(f32[1024,2048]{1,0:T(8,128)S(1)} %fusion.5, bf16[1024,448]{0,1:T(8,128)(2,1)S(1)} %get-tuple-element.71, bf16[1,2048,448]{1,2,0:T(8,128)(2,1)S(1)} %copy-done.9), kind=kOutput, calls=%fused_computation.4 | convolution fusion | flops 1881145344 | bytes 19529728 | tf_op jit(solution)/shard_map/dot_general | solution.py:230
  156.5 79.3 %reduce-scatter.2.cloned.1.call-done = f32[1024,512]{1,0:T(8,128)} async-done(((f32[1024,2048]{1,0:T(8,128)}), f32[1024,512]{1,0:T(8,128)}) %reduce-scatter.2.cloned.1.call-update) | async-done | bytes 2097168 | tf_op jit(solution)/shard_map/reduce_scatter | solution.py:309
  235.7 2.7 convert_element_type.100
  238.5 10.9 %all-to-all-start.1 = ((bf16[64,16,512]{2,1,0:T(8,128)(2,1)}), bf16[64,16,512]{2,1,0:T(8,128)(2,1)S(1)}, u32[]{:S(2)}, u32[]{:S(2)}) async-start(bf16[64,16,512]{2,1,0:T(8,128)(2,1)} %bitcast.12), calls=%async_computation.2 | async-start | bytes 2097152 | tf_op jit(solution)/shard_map/all_to_all | solution.py:310
  253.5 1.3 convolution_multiply_fusion.1
  254.9 5.8 %fusion.4 = bf16[1,2048,448]{1,2,0:T(8,128)(2,1)} fusion(bf16[1024,448]{0,1:T(8,128)(2,1)} %copy-done.8, bf16[1024,2048]{1,0:T(8,128)(2,1)} %bitcast.285), kind=kOutput, calls=%fused_computation.13 | convolution fusion | flops 1879965696 | bytes 6946816 | tf_op jit(solution)/shard_map/dot_general | solution.py:224
  260.7 16.9 %all-to-all-done.1 = bf16[64,16,512]{2,1,0:T(8,128)(2,1)S(1)} async-done(((bf16[64,16,512]{2,1,0:T(8,128)(2,1)}), bf16[64,16,512]{2,1,0:T(8,128)(2,1)S(1)}, u32[]{:S(2)}, u32[]{:S(2)}) %all-to-all-start.1) | async-done | bytes 1048608 | tf_op jit(solution)/shard_map/all_to_all | solution.py:310
  279.8 3.5 all-to-all-start.2
  283.4 5.6 %fusion.3 = bf16[1,2048,448]{1,2,0:T(8,128)(2,1)} fusion(bf16[1024,448]{0,1:T(8,128)(2,1)S(1)} %copy-done.49, bf16[1024,2048]{1,0:T(8,128)(2,1)} %bitcast.286), kind=kOutput, calls=%fused_computation.12 | convolution fusion | flops 1879965696 | bytes 6946816 | tf_op jit(solution)/shard_map/dot_general | solution.py:221
  289.0 3.4 fusion.2
  292.4 4.9 %all-to-all-done.2 = f32[4,128,512]{1,2,0:T(8,128)S(1)} async-done(((f32[4,128,512]{1,2,0:T(8,128)}), f32[4,128,512]{1,2,0:T(8,128)S(1)}, u32[]{:S(2)}, u32[]{:S(2)}) %all-to-all-start.2) | async-done | bytes 1048608 | tf_op jit(solution)/shard_map/all_to_all | solution.py:45
  300.2 3.6 all-gather.3
  304.0 1.7 fusion.94
  305.8 5.9 %all-to-all-start.3 = ((f32[64,32,256]{2,1,0:T(8,128)}), f32[64,32,256]{2,1,0:T(8,128)}, u32[]{:S(2)}, u32[]{:S(2)}) async-start(f32[64,32,256]{2,1,0:T(8,128)} %fusion.94), calls=%async_computation.4 | async-start | bytes 4194304 | tf_op jit(solution)/shard_map/all_to_all | solution.py:100
  313.9 13.6 %all-gather.4 = f32[4,257,64]{1,2,0:T(8,128)S(1)} all-gather(f32[1,257,64]{1,2,0:T(8,128)S(1)} %maximum_bitcast_fusion.1), channel_id=3, replica_groups=mesh['sp_0'=8,'sp_1'=4,'sp_2'=2,'tp'=4] {'sp_1'}, dimensions={0}, use_global_device_ids=true | all-gather | bytes 328960 | tf_op jit(solution)/shard_map/all_gather | solution.py:68
  329.5 46.1 %all-gather.5 = f32[8,257,64]{1,2,0:T(8,128)S(1)} all-gather(f32[1,257,64]{1,2,0:T(8,128)S(1)} %maximum_bitcast_fusion.2), channel_id=4, replica_groups=mesh['sp_0'=8,'sp_1'=4,'sp_2'=2,'tp'=4] {'sp_0'}, dimensions={0}, use_global_device_ids=true | all-gather | bytes 592128 | tf_op jit(solution)/shard_map/all_gather | solution.py:68
  376.8 1.1 fusion.45
  379.5 1.1 fusion.22
  380.6 1.4 convolution_multiply_fusion
  382.0 1.2 fusion.25
  384.4 2.3 reduce_sum.80
  (215 shorter events, 27.7 us)
Async XLA Ops:
  7.2 133.2 %copy-start = (bf16[1,2048,448]{1,2,0:T(8,128)(2,1)S(1)}, bf16[1,2048,448]{1,2,0:T(8,128)(2,1)}, u32[]{:S(2)}) copy-start(bf16[1,2048,448]{1,2,0:T(8,128)(2,1)} %param.21) | copy-start | bytes 5505028
  7.2 6.2 %copy-start.7 = (bf16[128,2048]{1,0:T(8,128)(2,1)S(1)}, bf16[128,2048]{1,0:T(8,128)(2,1)}, u32[]{:S(2)}) copy-start(bf16[128,2048]{1,0:T(8,128)(2,1)} %param.18) | copy-start | bytes 1572868
  7.2 228.5 %reduce-scatter.2.cloned.1.call-start = ((), (), s32[]{:S(2)}) async-start(), calls=%async_computation.5 | async-start | bytes 10485760 | tf_op jit(solution)/shard_map/reduce_scatter | solution.py:309
  125.6 6.2 %collective-permute-start = (bf16[64,8,2048]{2,1,0:T(8,128)(2,1)}, bf16[64,8,2048]{2,1,0:T(8,128)(2,1)}, u32[]{:S(2)}, u32[]{:S(2)}) collective-permute-start(bf16[64,8,2048]{2,1,0:T(8,128)(2,1)} %slice.210), channel_id=1, source_target_pairs={{0,4},{4,0},{8,12},{12,8},{16,20},{20,16},{24,28},{28,24},{32,36},... | collective-permute-start | bytes 6291464 | tf_op jit(solution)/shard_map/ppermute | solution.py:34
  135.0 4.4 %collective-permute-start.1 = (bf16[64,8,2048]{2,1,0:T(8,128)(2,1)S(1)}, bf16[64,8,2048]{2,1,0:T(8,128)(2,1)S(1)}, u32[]{:S(2)}, u32[]{:S(2)}) collective-permute-start(bf16[64,8,2048]{2,1,0:T(8,128)(2,1)S(1)} %get-tuple-element.70), channel_id=1, source_target_pairs={{0,4},{4,0},{8,12},{12,8},{16,20},{20,16},{24,28},{28,24},{32,36},... | collective-permute-start | bytes 6291464 | tf_op jit(solution)/shard_map/ppermute | solution.py:34
  136.0 9.4 %copy-start.4 = (bf16[64,16,2048]{2,1,0:T(8,128)(2,1)}, bf16[64,16,2048]{2,1,0:T(8,128)(2,1)S(1)}, u32[]{:S(2)}) copy-start(bf16[64,16,2048]{2,1,0:T(8,128)(2,1)S(1)} %pad_maximum_fusion.1) | copy-start | bytes 12582916
  238.4 11.2 %copy-start.47 = (f32[4]{0:T(128)S(1)}, f32[4]{0:T(128)}, u32[]{:S(2)}) copy-start(f32[4]{0:T(128)} %param.27) | copy-start | bytes 52
  238.4 11.2 %copy-start.27 = (f32[4,128]{1,0:T(4,128)S(1)}, f32[4,128]{1,0:T(4,128)}, u32[]{:S(2)}) copy-start(f32[4,128]{1,0:T(4,128)} %param.26) | copy-start | bytes 6148
  238.4 12.6 %copy-start.34 = (bf16[128,64]{0,1:T(8,128)(2,1)S(1)}, bf16[128,64]{0,1:T(8,128)(2,1)}, u32[]{:S(2)}) copy-start(bf16[128,64]{0,1:T(8,128)(2,1)} %param.29) | copy-start | bytes 49156
  238.4 12.6 %copy-start.35 = (bf16[128,64]{0,1:T(8,128)(2,1)S(1)}, bf16[128,64]{0,1:T(8,128)(2,1)}, u32[]{:S(2)}) copy-start(bf16[128,64]{0,1:T(8,128)(2,1)} %param.28) | copy-start | bytes 49156
  238.4 12.6 %copy-start.23 = (bf16[128,256]{1,0:T(8,128)(2,1)S(1)}, bf16[128,256]{1,0:T(8,128)(2,1)}, u32[]{:S(2)}) copy-start(bf16[128,256]{1,0:T(8,128)(2,1)} %param.24) | copy-start | bytes 196612
  238.5 12.7 %copy-start.24 = (bf16[128,256]{1,0:T(8,128)(2,1)S(1)}, bf16[128,256]{1,0:T(8,128)(2,1)}, u32[]{:S(2)}) copy-start(bf16[128,256]{1,0:T(8,128)(2,1)} %param.25) | copy-start | bytes 196612
  238.5 14.1 %copy-start.12 = (f32[1,4,64,64]{3,2,1,0:T(8,128)S(1)}, f32[1,4,64,64]{3,2,1,0:T(8,128)}, u32[]{:S(2)}) copy-start(f32[1,4,64,64]{3,2,1,0:T(8,128)} %param.30) | copy-start | bytes 196612
  238.5 39.0 %all-to-all-start.1 = ((bf16[64,16,512]{2,1,0:T(8,128)(2,1)}), bf16[64,16,512]{2,1,0:T(8,128)(2,1)S(1)}, u32[]{:S(2)}, u32[]{:S(2)}) async-start(bf16[64,16,512]{2,1,0:T(8,128)(2,1)} %bitcast.12), calls=%async_computation.2 | async-start | bytes 2097152 | tf_op jit(solution)/shard_map/all_to_all | solution.py:310
  250.1 10.6 %copy-start.30 = (f32[4,128]{1,0:T(4,128)}, f32[4,128]{1,0:T(4,128)S(1)}, u32[]{:S(2)}) copy-start(f32[4,128]{1,0:T(4,128)S(1)} %reduce_window_sum.29) | copy-start | bytes 6148
  251.0 9.6 %copy-start.14 = (f32[128,64]{0,1:T(8,128)}, f32[128,64]{0,1:T(8,128)S(1)}, u32[]{:S(2)}) copy-start(f32[128,64]{0,1:T(8,128)S(1)} %convert_element_type.107) | copy-start | bytes 98308
  251.0 9.6 %copy-start.19 = (f32[128,64]{0,1:T(8,128)}, f32[128,64]{0,1:T(8,128)S(1)}, u32[]{:S(2)}) copy-start(f32[128,64]{0,1:T(8,128)S(1)} %convert_element_type.108) | copy-start | bytes 98308
  251.9 8.7 %copy-start.25 = (pred[128,128]{1,0:T(8,128)(4,1)}, pred[128,128]{1,0:T(8,128)(4,1)S(1)}, u32[]{:S(2)}) copy-start(pred[128,128]{1,0:T(8,128)(4,1)S(1)} %iota_compare_fusion.2) | copy-start | bytes 49156
  252.6 47.1 %copy-start.31 = (f32[128,4]{0,1:T(4,128)}, f32[128,4]{0,1:T(4,128)S(1)}, u32[]{:S(2)}) copy-start(f32[128,4]{0,1:T(4,128)S(1)} %get-tuple-element.99) | copy-start | bytes 6148
  277.7 5.6 %copy-start.49 = (bf16[1024,448]{0,1:T(8,128)(2,1)S(1)}, bf16[1024,448]{0,1:T(8,128)(2,1)}, u32[]{:S(2)}) copy-start(bf16[1024,448]{0,1:T(8,128)(2,1)} %copy-done.48) | copy-start | bytes 2752516
  279.8 17.5 %all-to-all-start.2 = ((f32[4,128,512]{1,2,0:T(8,128)}), f32[4,128,512]{1,2,0:T(8,128)S(1)}, u32[]{:S(2)}, u32[]{:S(2)}) async-start(f32[4,128,512]{1,2,0:T(8,128)} %broadcast_in_dim.98), calls=%async_computation.3 | async-start | bytes 2097152 | tf_op jit(solution)/shard_map/all_to_all | solution.py:45
  283.3 5.7 %copy-start.5 = (bf16[64,16,2048]{2,1,0:T(8,128)(2,1)S(1)}, bf16[64,16,2048]{2,1,0:T(8,128)(2,1)}, u32[]{:S(2)}) copy-start(bf16[64,16,2048]{2,1,0:T(8,128)(2,1)} %copy-done.4) | copy-start | bytes 12582916
  283.3 5.7 %copy-start.51 = (f32[1024,448]{0,1:T(8,128)S(1)}, f32[1024,448]{0,1:T(8,128)}, u32[]{:S(2)}) copy-start(f32[1024,448]{0,1:T(8,128)} %copy-done.50) | copy-start | bytes 5505028
  283.3 5.7 %copy-start.53 = (f32[1024,448]{0,1:T(8,128)S(1)}, f32[1024,448]{0,1:T(8,128)}, u32[]{:S(2)}) copy-start(f32[1024,448]{0,1:T(8,128)} %copy-done.52) | copy-start | bytes 5505028
  289.0 8.7 %copy-start.45 = (f32[128]{0:T(128)S(1)}, f32[128]{0:T(128)}, u32[]{:S(2)}) copy-start(f32[128]{0:T(128)} %copy-done.44) | copy-start | bytes 1540
  289.0 8.7 %copy-start.42 = (f32[128]{0:T(128)S(1)}, f32[128]{0:T(128)}, u32[]{:S(2)}) copy-start(f32[128]{0:T(128)} %copy-done.41) | copy-start | bytes 1540
  303.9 9.4 %copy-start.43 = (f32[4]{0:T(128)}, f32[4]{0:T(128)S(1)}, u32[]{:S(2)}) copy-start(f32[4]{0:T(128)S(1)} %slice_bitcast_fusion.10) | copy-start | bytes 52
  303.9 9.3 %copy-start.37 = (f32[4]{0:T(128)}, f32[4]{0:T(128)S(1)}, u32[]{:S(2)}) copy-start(f32[4]{0:T(128)S(1)} %get-tuple-element.104) | copy-start | bytes 52
  305.8 78.7 %all-to-all-start.3 = ((f32[64,32,256]{2,1,0:T(8,128)}), f32[64,32,256]{2,1,0:T(8,128)}, u32[]{:S(2)}, u32[]{:S(2)}) async-start(f32[64,32,256]{2,1,0:T(8,128)} %fusion.94), calls=%async_computation.4 | async-start | bytes 4194304 | tf_op jit(solution)/shard_map/all_to_all | solution.py:100
  376.8 6.6 %copy-start.16 = (f32[128,64]{0,1:T(8,128)S(1)}, f32[128,64]{0,1:T(8,128)}, u32[]{:S(2)}) copy-start(f32[128,64]{0,1:T(8,128)} %copy-done.14) | copy-start | bytes 98308
  378.0 5.3 %copy-start.29 = (f32[4,128]{1,0:T(4,128)S(1)}, f32[4,128]{1,0:T(4,128)}, u32[]{:S(2)}) copy-start(f32[4,128]{1,0:T(4,128)} %param.26) | copy-start | bytes 6148
  378.8 8.0 %copy-start.1 = (bf16[1,2048,448]{1,2,0:T(8,128)(2,1)S(1)}, bf16[1,2048,448]{1,2,0:T(8,128)(2,1)}, u32[]{:S(2)}) copy-start(bf16[1,2048,448]{1,2,0:T(8,128)(2,1)} %param.21) | copy-start | bytes 5505028
  (28 other events, 62.0 us)
Sparse Core Ops, SparseCore 0:
  156.6 79.1 reduce-scatter.1
where the time goes:
time: 398 us; the launch traced here: 394 us
  blocking collectives  171 us (43%)
  waiting for transfers between devices  109 us (27%)
  matrix products  43.6 us (11%)
  starting transfers between devices  23 us (6%)
  local copies, waits for them, and re-layouts  16.8 us (4%)
  other arithmetic  15.7 us (4%)
  between operations  15.1 us (4%)
    all_to_all x1, blocking collectives, side_by_side(): lax.all_to_all(both, axis, split_axis=split_dim, concat_axis=concat_dim,...  107 us
    reduce_scatter x1, waiting for transfers between devices, shards(): lax.psum_scatter(input_part, 'tp', scatter_dimension=1, tiled=True)  79.3 us
    all_gather x3, blocking collectives, all_in_one(): both, at, found = (lax.all_gather(jnp.concatenate(lines), axis), 0, {})  63.3 us
    all_to_all x1, waiting for transfers between devices, shards(): lax.all_to_all(input_quarter.reshape(sp_count, capacity, quarter).astype(...  16.9 us
    all_to_all x1, starting transfers between devices, shards(): lax.all_to_all(input_quarter.reshape(sp_count, capacity, quarter).astype(...  10.9 us
  transfers between devices with their start and end apart: 6, of which 5 were waited for; matrix products, arithmetic and copies ran while one was open for 8% of the time, Pallas kernels for 0%

commit v1 on v0

v1 whole, which is shorter than its diff:
```python
import jax
import jax.numpy as jnp
from jax import lax
from jax.experimental import pallas as pl
from jax.experimental.pallas import tpu as pltpu
from jax.sharding import Mesh
from jax.sharding import PartitionSpec as P

D = 2048
HEADS = 16
STATE = 64
GROUPS = 4
SP = ("sp_0", "sp_1", "sp_2")


EPS = 1e-06
HIGHEST = lax.Precision.HIGHEST


MESH = pl.DeviceIdType.MESH
NZ, NX, NC, NY = 8, 4, 2, 4
CHIPS = NZ * NX
CAP = 16
HALF = CHIPS * CAP
QUARTER = 512


def position():
    return tuple(lax.axis_index(a) for a in ("sp_0", "sp_1", "sp_2", "tp"))


def at(z, x, c, y):
    return {"sp_0": z, "sp_1": x, "sp_2": c, "tp": y}


def remote(src, dst, send, recv, device):
    return pltpu.make_async_remote_copy(
        src_ref=src,
        dst_ref=dst,
        send_sem=send,
        recv_sem=recv,
        device_id=device,
        device_id_type=MESH,
    )


def signal(sem, device):
    pl.semaphore_signal(sem, inc=1, device_id=device, device_id_type=MESH)


def plane_peer(z, x, d):
    return lax.rem(z + d // NX, NZ), lax.rem(x + d % NX, NX)


def greet(z, x, c, y):
    barrier = pltpu.get_barrier_semaphore()

    def hello(d, carry):
        pz, px = plane_peer(z, x, d)
        signal(barrier, at(pz, px, c, y))
        return carry

    lax.fori_loop(1, CHIPS, hello, 0)
    signal(barrier, at(z, x, 1 - c, y))
    signal(barrier, at(z, x, c, lax.rem(y + 1, NY)))
    signal(barrier, at(z, x, c, lax.rem(y + 3, NY)))
    pl.semaphore_wait(barrier, CHIPS + 2)


CHUNKS = ((0, 0), (0, 1), (1, 0), (1, 1))
WIDE = QUARTER // 2


def dispatch_kernel(
    in_ref, cot_ref, gated_ref, rin_ref, rcot_ref, gz_ref, s1, r1, own_sem, sy, ry, sm, rm, sg, rg
):
    z, x, c, y = position()
    chip = z * NX + x
    up, down, far = lax.rem(y + 1, NY), lax.rem(y + 3, NY), lax.rem(y + 2, NY)
    greet(z, x, c, y)
    sources, targets = (in_ref, cot_ref), (rin_ref, rcot_ref)

    def cols(q, part):
        return pl.ds(pl.multiple_of(q * QUARTER + part * WIDE, WIDE), WIDE)

    def block(k, row, rows, q):
        array, part = CHUNKS[k]
        return targets[array].at[pl.ds(pl.multiple_of(row, CAP), rows), cols(q, part)]

    for k, (array, part) in enumerate(CHUNKS):
        local = pltpu.make_async_copy(
            sources[array].at[
                pl.ds(pl.multiple_of(chip * CAP, CAP), CAP), pl.ds(part * WIDE, WIDE)
            ],
            block(k, c * HALF + chip * CAP, CAP, y),
            own_sem.at[k],
        )
        local.start()

        def spread(d, carry):
            pz, px = plane_peer(z, x, d)
            peer = pz * NX + px
            remote(
                sources[array].at[
                    pl.ds(pl.multiple_of(peer * CAP, CAP), CAP), pl.ds(part * WIDE, WIDE)
                ],
                block(k, c * HALF + chip * CAP, CAP, y),
                s1.at[k],
                r1.at[k],
                at(pz, px, c, y),
            ).start()
            return carry

        lax.fori_loop(1, CHIPS, spread, 0)

    tokens_rows = gated_ref.shape[0]

    def gated_block(owner):
        return gz_ref.at[pl.ds(pl.multiple_of(owner * tokens_rows, 16), tokens_rows), :]

    gated_own = pltpu.make_async_copy(gated_ref, gated_block(z), own_sem.at[len(CHUNKS)])
    gated_own.start()

    def spread_gated(d, carry):
        remote(gated_ref, gated_block(z), sg, rg, at(lax.rem(z + d, NZ), x, c, y)).start()
        return carry

    lax.fori_loop(1, NZ, spread_gated, 0)

    mine, other = c * HALF, (1 - c) * HALF
    short = HALF - CAP
    part_rows = HALF // 2
    last = len(CHUNKS) - 1

    def relay(k, row, rows, q, slot):
        return remote(
            block(k, row, rows, q),
            block(k, row, rows, q),
            sm.at[k, slot],
            rm.at[k, slot],
            at(z, x, 1 - c, y),
        )

    def along(k, row, rows, q, slot, target):
        return remote(
            block(k, row, rows, q),
            block(k, row, rows, q),
            sy.at[k, slot],
            ry.at[k, slot],
            at(z, x, c, target),
        )

    def first(k):
        remote(
            block(k, 0, short, y), block(k, 0, short, y), s1.at[k], r1.at[k], at(z, x, c, up)
        ).wait_recv()
        pltpu.make_async_copy(
            block(k, 0, CAP, y), block(k, 0, CAP, y), own_sem.at[k]
        ).wait()
        along(k, mine, HALF, y, 0, up).start()
        along(k, mine, HALF, y, 1, down).start()
        relay(k, mine, HALF, y, 0).start()

    def second(k):
        along(k, mine, HALF, down, 0, up).wait_recv()
        along(k, mine, part_rows, down, 2, up).start()
        relay(k, mine, HALF, down, 1).start()
        along(k, mine, HALF, up, 1, down).wait_recv()
        along(k, mine + part_rows, part_rows, up, 3, down).start()
        relay(k, mine, HALF, up, 2).start()

    def third(k):
        along(k, mine, part_rows, far, 2, up).wait_recv()
        along(k, mine + part_rows, part_rows, far, 3, down).wait_recv()
        relay(k, mine, HALF, far, 3).start()

    for k in range(last + 1):
        first(k)
        if k >= 1:
            second(k - 1)
        if k >= 2:
            third(k - 2)
    second(last)
    third(last - 1)
    third(last)
    for k in range(last + 1):
        remote(
            block(k, 0, short, y), block(k, 0, short, y), s1.at[k], r1.at[k], at(z, x, c, up)
        ).wait_send()
        along(k, mine, HALF, y, 0, up).wait_send()
        along(k, mine, HALF, y, 1, down).wait_send()
        along(k, mine, part_rows, down, 2, up).wait_send()
        along(k, mine + part_rows, part_rows, up, 3, down).wait_send()
        for slot, q in enumerate((y, down, up, far)):
            relay(k, mine, HALF, q, slot).wait_send()
            relay(k, other, HALF, q, slot).wait_recv()
    gated_own.wait()
    seven = gz_ref.at[pl.ds(0, (NZ - 1) * tokens_rows), :]
    remote(seven, seven, sg, rg, at(z, x, c, up)).wait()


def dispatch(rows_in, rows_cot, gated):
    dma = pltpu.SemaphoreType.DMA
    n = len(CHUNKS)
    vmem, hbm = pl.BlockSpec(memory_space=pltpu.VMEM), pl.BlockSpec(memory_space=pl.ANY)
    return pl.pallas_call(
        dispatch_kernel,
        out_shape=(
            jax.ShapeDtypeStruct((2 * HALF, D), jnp.bfloat16),
            jax.ShapeDtypeStruct((2 * HALF, D), jnp.bfloat16),
            jax.ShapeDtypeStruct((NZ * gated.shape[0], gated.shape[1]), jnp.bfloat16),
        ),
        in_specs=[vmem] * 3,
        out_specs=(hbm, hbm, hbm),
        scratch_shapes=[
            dma((n,)),
            dma((n,)),
            dma((n + 1,)),
            dma((n, 4)),
            dma((n, 4)),
            dma((n, 4)),
            dma((n, 4)),
            dma,
            dma,
        ],
        compiler_params=pltpu.CompilerParams(collective_id=0, has_side_effects=True),
        name="dispatch",
    )(rows_in, rows_cot, gated)


def add_rows(target, t0, t1, pieces, step=64):
    rows = pieces[0][1]

    def body(i, carry):
        total = None
        for ref, _, r0, c0, width in pieces:
            value = ref[pl.ds(pl.multiple_of(r0 + i * step, 16), step), pl.ds(c0, width)].astype(
                jnp.float32
            )
            total = value if total is None else total + value
        target[
            pl.ds(pl.multiple_of(t0 + i * step, 16), step), pl.ds(t1, pieces[0][4])
        ] = total.astype(target.dtype)
        return carry

    lax.fori_loop(0, rows // step, body, 0)


def combine_kernel(
    part_ref, place_ref, out_ref, mate, acc, fwd, got, done, back, rows_out, sm, rm, sy, ry, sb, rb,
    sg, rg,
):
    z, x, c, y = position()
    chip = z * NX + x
    up, down, far = lax.rem(y + 1, NY), lax.rem(y + 3, NY), lax.rem(y + 2, NY)
    greet(z, x, c, y)
    mine, other = c * HALF, (1 - c) * HALF
    half = HALF // 2

    def cols(q):
        return pl.ds(pl.multiple_of(q * QUARTER, QUARTER), QUARTER)

    def rows(r0, n):
        return pl.ds(pl.multiple_of(r0, CAP), n)

    order = (far, up, down, y)
    for slot, q in enumerate(order):
        remote(
            part_ref.at[rows(other, HALF), cols(q)],
            mate.at[slot],
            sm.at[slot],
            rm.at[slot],
            at(z, x, 1 - c, y),
        ).start()

    def fold(slot):
        q = order[slot]
        remote(
            part_ref.at[rows(other, HALF), cols(q)],
            mate.at[slot],
            sm.at[slot],
            rm.at[slot],
            at(z, x, 1 - c, y),
        ).wait_recv()
        base = pl.multiple_of(q * QUARTER, QUARTER)

        def body(i, carry):
            at_rows = pl.ds(pl.multiple_of(i * 64, 64), 64)
            own = part_ref[
                pl.ds(pl.multiple_of(mine + i * 64, 64), 64), pl.ds(base, QUARTER)
            ].astype(jnp.float32)
            acc[slot, at_rows, :] = (own + mate[slot, at_rows, :].astype(jnp.float32)).astype(
                jnp.bfloat16
            )
            return carry

        lax.fori_loop(0, HALF // 64, body, 0)

    def along(src, dst, slot, target):
        return remote(src, dst, sy.at[slot], ry.at[slot], at(z, x, c, target))

    lo, hi = pl.ds(0, half), pl.ds(half, half)
    fold(0)
    f_up = along(acc.at[0, lo], fwd.at[0], 0, up)
    f_down = along(acc.at[0, hi], fwd.at[1], 1, down)
    f_up.start()
    f_down.start()
    fold(1)
    d_up = along(acc.at[1, hi], got.at[0, hi], 2, up)
    d_up.start()
    fold(2)
    d_down = along(acc.at[2, lo], got.at[1, lo], 3, down)
    d_down.start()

    def pass_on(slot, start, index):
        def body(i, carry):
            at_rows = pl.ds(pl.multiple_of(start + i * 64, 64), 64)
            from_rows = pl.ds(pl.multiple_of(i * 64, 64), 64)
            acc[slot, at_rows, :] = (
                acc[slot, at_rows, :].astype(jnp.float32)
                + fwd[index, from_rows, :].astype(jnp.float32)
            ).astype(jnp.bfloat16)
            return carry

        lax.fori_loop(0, half // 64, body, 0)

    f_up.wait_recv()
    pass_on(1, 0, 0)
    a_up = along(acc.at[1, lo], got.at[0, lo], 4, up)
    a_up.start()
    f_down.wait_recv()
    pass_on(2, half, 1)
    a_down = along(acc.at[2, hi], got.at[1, hi], 5, down)
    a_down.start()
    fold(3)
    d_up.wait_recv()
    d_down.wait_recv()

    def finish(start):
        def body(i, carry):
            at_rows = pl.ds(pl.multiple_of(start + i * 64, 64), 64)
            done[at_rows, :] = (
                acc[3, at_rows, :].astype(jnp.float32)
                + got[0, at_rows, :].astype(jnp.float32)
                + got[1, at_rows, :].astype(jnp.float32)
            ).astype(jnp.bfloat16)
            return carry

        lax.fori_loop(0, half // 64, body, 0)

    a_up.wait_recv()
    finish(0)
    a_down.wait_recv()
    finish(half)

    own_rows = pl.ds(pl.multiple_of(chip * CAP, CAP), CAP)

    def give_back(d, carry):
        pz, px = plane_peer(z, x, d)
        remote(
            done.at[rows((pz * NX + px) * CAP, CAP), :],
            back.at[own_rows, :],
            sb,
            rb,
            at(pz, px, c, y),
        ).start()
        return carry

    lax.fori_loop(1, CHIPS, give_back, 0)
    back[own_rows, :] = done[own_rows, :]
    short = pl.ds(0, HALF - CAP)
    all_back = remote(done.at[short, :], back.at[short, :], sb, rb, at(z, x, c, up))
    all_back.wait_recv()
    rows_out[y] = jnp.dot(
        place_ref[...], back[...], preferred_element_type=jnp.float32
    ).astype(jnp.bfloat16)
    n = rows_out.shape[1]
    first, second = pl.ds(0, n // 2), pl.ds(n // 2, n // 2)

    def share(q, piece, slot, target):
        return remote(
            rows_out.at[q, piece], rows_out.at[q, piece], sg.at[slot], rg.at[slot], at(z, x, c, target)
        )

    everything = pl.ds(0, n)
    share(y, everything, 0, up).start()
    share(y, everything, 1, down).start()
    share(down, everything, 0, up).wait_recv()
    share(down, first, 2, up).start()
    share(up, everything, 1, down).wait_recv()
    share(up, second, 3, down).start()
    out_ref[:, cols(y)] = rows_out[y]
    out_ref[:, cols(down)] = rows_out[down]
    out_ref[:, cols(up)] = rows_out[up]
    share(far, first, 2, up).wait_recv()
    share(far, second, 3, down).wait_recv()
    out_ref[:, cols(far)] = rows_out[far]
    for slot, q in enumerate(order):
        remote(
            part_ref.at[rows(other, HALF), cols(q)],
            mate.at[slot],
            sm.at[slot],
            rm.at[slot],
            at(z, x, 1 - c, y),
        ).wait_send()
    for copy in (f_up, f_down, d_up, d_down, a_up, a_down, all_back):
        copy.wait_send()
    share(y, everything, 0, up).wait_send()
    share(y, everything, 1, down).wait_send()
    share(down, first, 2, up).wait_send()
    share(up, second, 3, down).wait_send()


def combine(parts, place):
    dma = pltpu.SemaphoreType.DMA
    vmem = pl.BlockSpec(memory_space=pltpu.VMEM)
    tok_rows = place.shape[0]
    bf16 = jnp.bfloat16
    return pl.pallas_call(
        combine_kernel,
        out_shape=jax.ShapeDtypeStruct((tok_rows, D), bf16),
        in_specs=[vmem] * 2,
        out_specs=vmem,
        scratch_shapes=[
            pltpu.VMEM((NY, HALF, QUARTER), bf16),
            pltpu.VMEM((NY, HALF, QUARTER), bf16),
            pltpu.VMEM((2, HALF // 2, QUARTER), bf16),
            pltpu.VMEM((2, HALF, QUARTER), bf16),
            pltpu.VMEM((HALF, QUARTER), bf16),
            pltpu.VMEM((HALF, QUARTER), bf16),
            pltpu.VMEM((NY, tok_rows, QUARTER), bf16),
            dma((NY,)),
            dma((NY,)),
            dma((6,)),
            dma((6,)),
            dma,
            dma,
            dma((4,)),
            dma((4,)),
        ],
        compiler_params=pltpu.CompilerParams(collective_id=1, has_side_effects=True),
        name="combine",
    )(parts, place)


ROWS8 = 16
MESSAGE = 24


def carry_kernel(
    msg_ref, res_ref, gated_ref, later_ref, opg_ref, box_a, plane, box_b, fan, res_box, prod,
    opg_box, sa, ra, sb, rb, sc, rc, sr, rr, so, ro,
):
    z, x, c, y = position()
    w = x * NC + c
    barrier = pltpu.get_barrier_semaphore()

    def in_plane(d):
        p = lax.rem(w + d, NX * NC)
        return p, at(z, p // NC, p % NC, y)

    def in_line(d):
        p = lax.rem(z + d, NZ)
        return p, at(p, x, c, y)

    for d in range(1, 8):
        signal(barrier, in_plane(d)[1])
        signal(barrier, in_line(d)[1])
    pl.semaphore_wait(barrier, 14)

    for d in range(1, 8):
        p, device = in_plane(d)
        remote(msg_ref.at[p], box_a.at[w], sa.at[d], ra.at[d], device).start()
    box_a[w] = msg_ref[w]
    for d in range(1, 8):
        p, device = in_plane(d)
        source = lax.rem(w + 8 - d, 8)
        remote(msg_ref.at[p], box_a.at[source], sa.at[d], ra.at[d], device).wait_recv()

    data, scale = pl.ds(0, ROWS8), pl.ds(ROWS8, 8)

    def pair(ref, i):
        s = ref[i, scale, :]
        return ref[i, data, :], jnp.concatenate([s, s], axis=0)

    total = jnp.zeros((ROWS8, 128), jnp.float32)
    decay = jnp.ones((ROWS8, 128), jnp.float32)
    inside, inside_decay = [], []
    for k in reversed(range(8)):
        inside.append(total)
        inside_decay.append(decay)
        value, factor = pair(box_a, k)
        total = value + factor * total
        decay = factor * decay
    inside, inside_decay = inside[::-1], inside_decay[::-1]
    plane[data, :] = total
    plane[scale, :] = decay[0:8, :]
    box_b[z, data, :] = total
    box_b[z, scale, :] = decay[0:8, :]
    for d in range(1, 8):
        p, device = in_line(d)
        remote(plane, box_b.at[z], sb.at[d], rb.at[d], device).start()

    def feature_cols(p):
        return pl.ds(pl.multiple_of(p * 256, 256), 256)

    for d in range(1, 8):
        p, device = in_line(d)
        remote(res_ref.at[:, feature_cols(p)], res_box.at[z], sr.at[d], rr.at[d], device).start()
    for d in range(1, 8):
        p, device = in_line(d)
        source = lax.rem(z + 8 - d, 8)
        remote(plane, box_b.at[source], sb.at[d], rb.at[d], device).wait_recv()
    beyond = jnp.zeros((ROWS8, 128), jnp.float32)
    for k in reversed(range(1, 8)):
        value, factor = pair(box_b, k)
        beyond = jnp.where(k > z, value + factor * beyond, beyond)
    for k in range(8):
        fan[k] = inside[k] + inside_decay[k] * beyond

    def own_rows(p):
        return pl.ds(pl.multiple_of(p * ROWS8, ROWS8), ROWS8)

    for d in range(1, 8):
        p, device = in_plane(d)
        remote(fan.at[p], later_ref.at[own_rows(w), :], sc.at[d], rc.at[d], device).start()
    later_ref[own_rows(w), :] = fan[w]

    res_box[z] = res_ref[:, feature_cols(z)]
    for d in range(1, 8):
        p, device = in_line(d)
        source = lax.rem(z + 8 - d, 8)
        remote(
            res_ref.at[:, feature_cols(p)], res_box.at[source], sr.at[d], rr.at[d], device
        ).wait_recv()
    n = res_ref.shape[0]
    value = None
    for k in range(8):
        term = lax.dot_general(
            res_box[k],
            gated_ref[pl.ds(k * n, n), :],
            (((0,), (0,)), ((), ())),
            preferred_element_type=jnp.float32,
        )
        value = term if value is None else value + term
    prod[...] = value.reshape(prod.shape)
    for d in range(1, 8):
        p, device = in_plane(d)
        remote(prod.at[p], opg_box.at[w], so.at[d], ro.at[d], device).start()
    opg_box[w] = prod[w]
    for d in range(1, 8):
        p, device = in_plane(d)
        source = lax.rem(w + 8 - d, 8)
        remote(prod.at[p], opg_box.at[source], so.at[d], ro.at[d], device).wait_recv()
    opg = opg_box[0]
    for k in range(1, 8):
        opg = opg + opg_box[k]
    opg_ref[...] = opg
    for d in range(1, 8):
        p, device = in_plane(d)
        source = lax.rem(w + 8 - d, 8)
        remote(fan.at[p], later_ref.at[own_rows(source), :], sc.at[d], rc.at[d], device).wait_recv()
        remote(msg_ref.at[p], box_a.at[w], sa.at[d], ra.at[d], device).wait_send()
        remote(fan.at[p], later_ref.at[own_rows(w), :], sc.at[d], rc.at[d], device).wait_send()
        remote(prod.at[p], opg_box.at[w], so.at[d], ro.at[d], device).wait_send()
        p, device = in_line(d)
        remote(plane, box_b.at[z], sb.at[d], rb.at[d], device).wait_send()
        remote(
            res_ref.at[:, feature_cols(p)], res_box.at[z], sr.at[d], rr.at[d], device
        ).wait_send()


def exchange_carry(messages, residual_grad, gated_line):
    dma = pltpu.SemaphoreType.DMA
    vmem = pl.BlockSpec(memory_space=pltpu.VMEM)
    f32 = jnp.float32
    n, channels = residual_grad.shape[0], gated_line.shape[1]
    return pl.pallas_call(
        carry_kernel,
        out_shape=(
            jax.ShapeDtypeStruct((128, 128), f32),
            jax.ShapeDtypeStruct((32, channels), f32),
        ),
        in_specs=[vmem] * 3,
        out_specs=(vmem, vmem),
        scratch_shapes=[
            pltpu.VMEM((8, MESSAGE, 128), f32),
            pltpu.VMEM((MESSAGE, 128), f32),
            pltpu.VMEM((8, MESSAGE, 128), f32),
            pltpu.VMEM((8, ROWS8, 128), f32),
            pltpu.VMEM((8, n, 256), jnp.bfloat16),
            pltpu.VMEM((8, 32, channels), f32),
            pltpu.VMEM((8, 32, channels), f32),
        ]
        + [dma((8,))] * 10,
        compiler_params=pltpu.CompilerParams(collective_id=2, has_side_effects=True),
        name="carry",
    )(messages, residual_grad, gated_line)


def prepare(scan_rows, step_rows, write_rows, read_rows, decay_rates, per_group):
    length = scan_rows.shape[0]
    head_count = step_rows.shape[0]
    logdec = jnp.cumsum(-decay_rates[:, None] * step_rows, axis=1)
    causal = jnp.arange(length)[:, None] >= jnp.arange(length)[None, :]
    spread = jnp.where(causal[None, :, :], logdec[:, :, None] - logdec[:, None, :], -jnp.inf)
    weights = jnp.exp(spread)
    inputs = (
        scan_rows.astype(jnp.float32).reshape(length, head_count, -1)
        * jnp.transpose(step_rows)[:, :, None]
    )
    write_head = jnp.repeat(
        write_rows.astype(jnp.float32).reshape(length, -1, STATE), per_group, axis=1
    )
    read_head = jnp.repeat(
        read_rows.astype(jnp.float32).reshape(length, -1, STATE), per_group, axis=1
    )
    scores = jnp.einsum("thn,shn->hts", read_head, write_head, precision=HIGHEST) * weights
    return (logdec, weights, inputs, write_head, read_head, scores)


def block_back(
    step_rows,
    logdec,
    weights,
    inputs,
    write_head,
    read_head,
    scores,
    entry_state,
    state_grad,
    later_state,
    per_group,
):
    length, head_count = (inputs.shape[0], inputs.shape[1])
    growth = jnp.transpose(jnp.exp(logdec))
    shrink = jnp.transpose(jnp.exp(logdec[:, -1:] - logdec))
    in_grad = jnp.einsum("hts,thp->shp", scores, state_grad, precision=HIGHEST)
    in_grad = in_grad + shrink[:, :, None] * jnp.einsum(
        "shn,hpn->shp", write_head, later_state, precision=HIGHEST
    )
    scan_grad = (
        (in_grad * jnp.transpose(step_rows)[:, :, None]).reshape(length, -1).astype(jnp.bfloat16)
    )
    pair_terms = jnp.einsum("thp,shp->hts", state_grad, inputs, precision=HIGHEST) * weights
    read_grad = jnp.einsum("hts,shn->thn", pair_terms, write_head, precision=HIGHEST)
    read_grad = read_grad + growth[:, :, None] * jnp.einsum(
        "thp,hpn->thn", state_grad, entry_state, precision=HIGHEST
    )
    write_grad = jnp.einsum("hts,thn->shn", pair_terms, read_head, precision=HIGHEST)
    write_grad = write_grad + shrink[:, :, None] * jnp.einsum(
        "shp,hpn->shn", inputs, later_state, precision=HIGHEST
    )
    group_count = head_count // per_group
    read_total = (
        jnp.sum(read_grad.reshape(length, group_count, per_group, -1), axis=2)
        .reshape(length, -1)
        .astype(jnp.bfloat16)
    )
    write_total = (
        jnp.sum(write_grad.reshape(length, group_count, per_group, -1), axis=2)
        .reshape(length, -1)
        .astype(jnp.bfloat16)
    )
    return (scan_grad, write_total, read_total)


def expert_grads(rows_in, rows_cot, gate_mat, up_mat, down_mat):
    contract_rows = (((0,), (0,)), ((), ()))
    contract_cols = (((1,), (1,)), ((), ()))
    gate_pre = jnp.dot(rows_in, gate_mat, preferred_element_type=jnp.float32)
    up_pre = jnp.dot(rows_in, up_mat, preferred_element_type=jnp.float32)
    sigmoid_val = jax.nn.sigmoid(gate_pre)
    active = (gate_pre * sigmoid_val * up_pre).astype(jnp.bfloat16)
    down_grad = lax.dot_general(active, rows_cot, contract_rows, preferred_element_type=jnp.float32)
    act_grad = lax.dot_general(
        rows_cot, down_mat, contract_cols, preferred_element_type=jnp.float32
    )
    gate_pre_grad = (
        act_grad * up_pre * sigmoid_val * (1.0 + gate_pre * (1.0 - sigmoid_val))
    ).astype(jnp.bfloat16)
    up_pre_grad = (act_grad * gate_pre * sigmoid_val).astype(jnp.bfloat16)
    gate_grad = lax.dot_general(
        rows_in, gate_pre_grad, contract_rows, preferred_element_type=jnp.float32
    )
    up_grad = lax.dot_general(
        rows_in, up_pre_grad, contract_rows, preferred_element_type=jnp.float32
    )
    input_grad = lax.dot_general(
        gate_pre_grad, gate_mat, contract_cols, preferred_element_type=jnp.float32
    )
    input_grad = input_grad + lax.dot_general(
        up_pre_grad, up_mat, contract_cols, preferred_element_type=jnp.float32
    )
    return (gate_grad, up_grad, down_grad, input_grad)


def shards(
    tokens,
    norm_gain,
    cotangent,
    routes,
    route_weight,
    gate_weight,
    up_weight,
    down_weight,
    scan_input,
    out_gate,
    step_size,
    decay_rate,
    write_keys,
    read_keys,
    start_state,
    out_proj,
):
    tok_rows = tokens.shape[0]
    experts_count = CHIPS
    y = lax.axis_index("tp")
    hidden = tokens.astype(jnp.float32)
    inverse = lax.rsqrt(jnp.mean(hidden * hidden, axis=1) + EPS)

    def quarter_of(a):
        return lax.dynamic_slice_in_dim(a, y * QUARTER, QUARTER, a.ndim - 1)

    normed_q = (
        quarter_of(tokens).astype(jnp.float32) * inverse[:, None] * quarter_of(norm_gain)[None, :]
    ).astype(jnp.bfloat16)
    cot_q = quarter_of(cotangent)
    route_flat = routes.reshape(-1)
    member = (route_flat[:, None] == jnp.arange(experts_count, dtype=jnp.int32)[None, :]).astype(
        jnp.int32
    )
    earlier_count = jnp.sum((jnp.cumsum(member, axis=0) - member) * member, axis=1)
    places = (route_flat * CAP + earlier_count).reshape(tok_rows, 2)
    slot_ids = jnp.arange(experts_count * CAP, dtype=jnp.int32)[:, None]
    first_hit = slot_ids == places[None, :, 0]
    second_hit = slot_ids == places[None, :, 1]
    placing = jnp.logical_or(first_hit, second_hit)
    place_matrix = placing.astype(jnp.bfloat16)
    slot_weight = jnp.sum(
        jnp.where(first_hit, route_weight[None, :, 0], 0.0)
        + jnp.where(second_hit, route_weight[None, :, 1], 0.0),
        axis=1,
    )
    send_in = jnp.dot(place_matrix, normed_q, preferred_element_type=jnp.float32).astype(
        jnp.bfloat16
    )
    send_cot = (
        slot_weight[:, None] * jnp.dot(place_matrix, cot_q, preferred_element_type=jnp.float32)
    ).astype(jnp.bfloat16)
    per_group = HEADS // GROUPS
    entry_state = start_state[0]
    logdec, weights, inputs, write_head, read_head, scores = prepare(
        scan_input, step_size, write_keys, read_keys, decay_rate, per_group
    )
    head_count = inputs.shape[1]
    growth = jnp.transpose(jnp.exp(logdec))
    scan_out = jnp.einsum("hts,shp->thp", scores, inputs, precision=HIGHEST)
    scan_out = scan_out + growth[:, :, None] * jnp.einsum(
        "thn,hpn->thp", read_head, entry_state, precision=HIGHEST
    )
    gate_val = out_gate.astype(jnp.float32).reshape(tok_rows, head_count, -1)
    sigmoid_val = jax.nn.sigmoid(gate_val)
    gated = (scan_out * gate_val * sigmoid_val).reshape(tok_rows, -1).astype(jnp.bfloat16)
    rows_in, rows_cot, gated_line = dispatch(send_in, send_cot, gated)
    gate_grad, up_grad, down_grad, input_part = expert_grads(
        rows_in, rows_cot, gate_weight[0], up_weight[0], down_weight[0]
    )
    normed_grad = combine(
        input_part.astype(jnp.bfloat16), jnp.transpose(place_matrix)
    ).astype(jnp.float32)
    gained = norm_gain[None, :] * normed_grad
    dotted = jnp.sum(hidden * gained, axis=1)
    residual = (
        cotangent.astype(jnp.float32)
        + inverse[:, None] * gained
        - hidden * (inverse**3 * dotted / D)[:, None]
    )
    residual_grad = residual.astype(jnp.bfloat16)
    mix_grad = jnp.dot(residual_grad, out_proj, preferred_element_type=jnp.float32)
    out_grad = mix_grad.reshape(tok_rows, head_count, -1)
    state_grad = out_grad * gate_val * sigmoid_val
    gate_out_grad = (
        (out_grad * scan_out * sigmoid_val * (1.0 + gate_val * (1.0 - sigmoid_val)))
        .reshape(tok_rows, -1)
        .astype(jnp.bfloat16)
    )
    carried = jnp.einsum("th,thp,thn->hpn", growth, state_grad, read_head, precision=HIGHEST)
    decay_now = jnp.exp(logdec[:, -1])
    messages = jnp.concatenate(
        [
            carried.reshape(8, ROWS8, 128),
            jnp.broadcast_to(jnp.repeat(decay_now, 2)[:, None, None], (8, 8, 128)),
        ],
        axis=1,
    )
    later, out_proj_grad = exchange_carry(messages, residual_grad, gated_line)
    later_state = later.reshape(head_count, 64, 64)
    scan_grad, write_grad, read_grad = block_back(
        step_size,
        logdec,
        weights,
        inputs,
        write_head,
        read_head,
        scores,
        entry_state,
        state_grad,
        later_state,
        per_group,
    )
    residual_part = quarter_of(residual_grad)
    return (
        residual_part,
        gate_grad.astype(jnp.bfloat16)[None],
        up_grad.astype(jnp.bfloat16)[None],
        down_grad.astype(jnp.bfloat16)[None],
        out_proj_grad,
        scan_grad,
        gate_out_grad,
        write_grad,
        read_grad,
    )


def solution(mesh):
    finer = Mesh(mesh.devices.reshape(8, 4, 2, mesh.shape["tp"]), ("sp_0", "sp_1", "sp_2", "tp"))
    in_specs = (
        P(SP, None),
        P(),
        P(SP, None),
        P(SP, None),
        P(SP, None),
        P(SP, None, "tp"),
        P(SP, None, "tp"),
        P(SP, "tp", None),
        P(SP, "tp"),
        P(SP, "tp"),
        P("tp", SP),
        P("tp"),
        P(SP, "tp"),
        P(SP, "tp"),
        P(SP, "tp", None, None),
        P(None, "tp"),
    )
    out_specs = (
        P(SP, "tp"),
        P(SP, None, "tp"),
        P(SP, None, "tp"),
        P(SP, "tp", None),
        P(SP, "tp"),
        P(SP, "tp"),
        P(SP, "tp"),
        P(SP, "tp"),
        P(SP, "tp"),
    )
    return jax.shard_map(
        shards, mesh=finer, in_specs=in_specs, out_specs=out_specs, check_vma=False
    )
```

time: 398 us -> 205 us (0.52)
  blocking collectives: 171 us -> 0 us
  Pallas kernels: 0 us -> 146 us
  waiting for transfers between devices: 109 us -> 0 us
  starting transfers between devices: 23 us -> 0 us
  between operations: 15.1 us -> 1.01 us
  local copies, waits for them, and re-layouts: 16.8 us -> 9.1 us
  matrix products: 43.6 us -> 37.6 us
  other arithmetic: 15.7 us -> 10.8 us
    pallas_call x0 -> x3, Pallas kernels: none -> 146 us  [the longest x1 60.6 us: dispatch(): pl.pallas_call(dispatch_kernel, out_shape=(jax.ShapeDtypeStruct((2 * HALF...]
    all_to_all x1 -> x0, blocking collectives: 107 us -> none  [side_by_side(): lax.all_to_all(both, axis, split_axis=split_dim, concat_axis=concat_dim,...]
    reduce_scatter x1 -> x0, waiting for transfers between devices: 79.3 us -> none  [shards(): lax.psum_scatter(input_part, 'tp', scatter_dimension=1, tiled=True)]
    all_gather x3 -> x0, blocking collectives: 63.3 us -> none  [all_in_one(): both, at, found = (lax.all_gather(jnp.concatenate(lines), axis), 0, {})]
    all_to_all x3 -> x0, waiting for transfers between devices: 21.8 us -> none  [the longest x1 16.9 us: shards(): lax.all_to_all(input_quarter.reshape(sp_count, capacity, quarter).astype(...]
    all_to_all x3 -> x0, starting transfers between devices: 20.3 us -> none  [the longest x1 10.9 us: shards(): lax.all_to_all(input_quarter.reshape(sp_count, capacity, quarter).astype(...]
    ppermute x2 -> x0, waiting for transfers between devices: 7.59 us -> none  [swapped(): return lax.ppermute(value, axis, pairs)]
    unnamed x115 -> x32, local copies, waits for them, and re-layouts: 7.88 us -> 3.03 us
  transfers between devices with their start and end apart: 6 -> 0, of which waited for: 5 -> 0; matrix products, arithmetic and copies ran while one was open for 8% -> 0% of each run, Pallas kernels for 0% -> 0%
where the time goes in v1:
time: 205 us; the launch traced here: 204 us
  Pallas kernels  146 us (71%)
  matrix products  37.6 us (18%)
  other arithmetic  10.8 us (5%)
  local copies, waits for them, and re-layouts  9.1 us (4%)
    pallas_call x1, Pallas kernels, dispatch(): pl.pallas_call(dispatch_kernel, out_shape=(jax.ShapeDtypeStruct((2 * HALF...  60.6 us
    pallas_call x1, Pallas kernels, combine(): pl.pallas_call(combine_kernel, out_shape=jax.ShapeDtypeStruct((tok_rows,...  50.8 us
    pallas_call x1, Pallas kernels, exchange_carry(): pl.pallas_call(carry_kernel, out_shape=(jax.ShapeDtypeStruct((128, 128),...  34.4 us
    dot_general x1, matrix products, expert_grads(): lax.dot_general(up_pre_grad, up_mat, contract_cols, preferred_element_typ...  4.55 us
    dot_general x1, matrix products, expert_grads(): gate_pre = jnp.dot(rows_in, gate_mat, preferred_element_type=jnp.float32)  4.43 us

profile of v1, /device:TPU:1, one launch (start us, length us, event | category | flops | bytes accessed | tf_op | source)
XLA Modules:
  0.0 204.3 jit_solution(9063369044844573914)
XLA Ops:
  0.7 1.4 fusion.25
  2.8 0.8 slice_bitcast_fusion.1
  3.6 0.8 broadcast_multiply_fusion
  5.0 0.8 dynamic_slice.13
  5.9 0.7 convert_element_type.95
  6.6 0.7 convert_element_type.96
  7.4 0.8 copy.72
  10.4 0.8 fusion.32.place_ref
  11.2 1.2 fusion.18
  12.4 0.9 copy.76
  14.1 1.3 multiply_convert_fusion.7
  15.4 0.7 copy.78.gated_ref
  16.1 2.0 fusion.12.cot_ref
  18.1 1.2 convolution_convert_fusion.3.in_ref
  19.3 60.6 %dispatch.1 = (bf16[1024,2048]{1,0:T(8,128)(2,1)}, bf16[1024,2048]{1,0:T(8,128)(2,1)}, bf16[1024,256]{1,0:T(8,128)(2,1)}) custom-call(bf16[512,512]{1,0:T(8,128)(2,1)} %convolution_convert_fusion.3.in_ref, bf16[512,512]{1,0:T(8,128)(2,1)} %fusion.12.cot_ref, bf16[128,256]{1,0:T(8,128)(2,1)} %copy.78.gated_ref), custom_call_target="tpu_custom_call" | custom-call | tf_op jit(solution)/shard_map/dispatch/pallas_call | solution.py:206
  79.9 4.4 %fusion.5 = f32[1024,448]{0,1:T(8,128)S(1)} fusion(bf16[1024,2048]{1,0:T(8,128)(2,1)} %get-tuple-element.15, bf16[1,2048,448]{1,2,0:T(8,128)(2,1)S(1)} %copy-done), kind=kOutput, calls=%fused_computation.9 | convolution fusion | flops 1879048192 | bytes 7864320 | tf_op jit(solution)/shard_map/dot_general | solution.py:671
  84.3 2.1 %fusion.8 = f32[1024,448]{0,1:T(8,128)S(1)} fusion(bf16[1024,2048]{1,0:T(8,128)(2,1)S(1)} %copy-done.10, bf16[1,2048,448]{1,2,0:T(8,128)(2,1)S(1)} %copy-done.13), kind=kOutput, calls=%fused_computation.12 | convolution fusion | flops 1879048192 | bytes 7864320 | tf_op jit(solution)/shard_map/dot_general | solution.py:672
  86.5 3.4 %fusion = bf16[1,448,2048]{2,1,0:T(8,128)(2,1)} fusion(bf16[1024,2048]{1,0:T(8,128)(2,1)S(1)} %copy-done.11, f32[1024,448]{0,1:T(8,128)S(1)} %fusion.8, f32[1024,448]{0,1:T(8,128)S(1)} %fusion.5), kind=kOutput, calls=%fused_computation.4 | convolution fusion | flops 1882718208 | bytes 9699328 | tf_op jit(solution)/shard_map/dot_general | solution.py:675
  89.9 2.6 %multiply_convert_fusion.1 = (bf16[1024,448]{0,1:T(8,128)(2,1)S(1)}, bf16[1024,448]{0,1:T(8,128)(2,1)S(1)}) fusion(f32[1024,448]{0,1:T(8,128)S(1)} %fusion.5, f32[1024,448]{0,1:T(8,128)S(1)} %fusion.8, bf16[1024,2048]{1,0:T(8,128)(2,1)S(1)} %copy-done.11, bf16[1,448,2048]{2,1,0:T(8,128)(2,1)S(1)} %copy-done.12), kind=kOutput, calls=%fused_computation.17 | convolution fusion | flops 1885011968 | bytes 11534336 | tf_op jit(solution)/shard_map/dot_general | solution.py:676
  92.5 3.3 %fusion.2 = bf16[1,2048,448]{1,2,0:T(8,128)(2,1)} fusion(bf16[1024,448]{0,1:T(8,128)(2,1)S(1)} %get-tuple-element.64, bf16[1024,2048]{1,0:T(8,128)(2,1)S(1)} %copy-done.10), kind=kOutput, calls=%fused_computation.6 | convolution fusion | flops 1879965696 | bytes 6946816 | tf_op jit(solution)/shard_map/dot_general | solution.py:686
  95.8 3.3 %fusion.1 = bf16[1,2048,448]{1,2,0:T(8,128)(2,1)} fusion(bf16[1024,448]{0,1:T(8,128)(2,1)S(1)} %get-tuple-element.65, bf16[1024,2048]{1,0:T(8,128)(2,1)S(1)} %copy-done.10), kind=kOutput, calls=%fused_computation.5 | convolution fusion | flops 1879965696 | bytes 6946816 | tf_op jit(solution)/shard_map/dot_general | solution.py:683
  99.1 2.7 %fusion.3 = f32[1024,2048]{1,0:T(8,128)S(1)} fusion(bf16[1024,448]{0,1:T(8,128)(2,1)S(1)} %get-tuple-element.65, bf16[1,2048,448]{1,2,0:T(8,128)(2,1)S(1)} %copy-done), kind=kOutput, calls=%fused_computation.7 | convolution fusion | flops 1879048192 | bytes 11141120 | tf_op jit(solution)/shard_map/dot_general | solution.py:689
  101.8 4.5 %add_convert_fusion.part_ref = bf16[1024,2048]{1,0:T(8,128)(2,1)} fusion(f32[1024,2048]{1,0:T(8,128)S(1)} %fusion.3, bf16[1024,448]{0,1:T(8,128)(2,1)S(1)} %get-tuple-element.64, bf16[1,2048,448]{1,2,0:T(8,128)(2,1)S(1)} %copy-done.13), kind=kOutput, calls=%fused_computation | convolution fusion | flops 1883242496 | bytes 15335424 | tf_op jit(solution)/shard_map/dot_general | solution.py:692
  106.4 50.8 %combine.1 = bf16[128,2048]{1,0:T(8,128)(2,1)} custom-call(bf16[1024,2048]{1,0:T(8,128)(2,1)} %add_convert_fusion.part_ref, bf16[128,512]{1,0:T(8,128)(2,1)} %fusion.32.place_ref), custom_call_target="tpu_custom_call" | custom-call | tf_op jit(solution)/shard_map/combine/pallas_call | solution.py:419
  157.2 1.4 fusion.26
  158.6 1.6 fusion.28.res_ref
  161.6 0.7 copy.83
  163.8 34.4 %carry.1 = (f32[128,128]{1,0:T(8,128)}, f32[32,256]{1,0:T(8,128)}) custom-call(f32[8,24,128]{2,1,0:T(8,128)} %pad_maximum_fusion.msg_ref, bf16[128,2048]{1,0:T(8,128)(2,1)} %copy-done.2, bf16[1024,256]{1,0:T(8,128)(2,1)} %get-tuple-element.16.gated_ref), custom_call_target="tpu_custom_call" | custom-call | tf_op jit(solution)/shard_map/carry/pallas_call | solution.py:578
  198.2 0.9 reshape.130
  200.8 1.2 fusion.24
  202.0 0.9 fusion.23
  202.9 0.7 copy.82
  (66 shorter events, 9.6 us)
Async XLA Ops:
  0.6 79.2 %copy-start = (bf16[1,2048,448]{1,2,0:T(8,128)(2,1)S(1)}, bf16[1,2048,448]{1,2,0:T(8,128)(2,1)}, u32[]{:S(2)}) copy-start(bf16[1,2048,448]{1,2,0:T(8,128)(2,1)} %param.21) | copy-start | bytes 5505028
  0.7 13.4 %copy-start.7 = (f32[4,128]{1,0:T(4,128)S(1)}, f32[4,128]{1,0:T(4,128)}, u32[]{:S(2)}) copy-start(f32[4,128]{1,0:T(4,128)} %param.26) | copy-start | bytes 6148
  0.7 12.7 %copy-start.6 = (bf16[128,256]{1,0:T(8,128)(2,1)S(1)}, bf16[128,256]{1,0:T(8,128)(2,1)}, u32[]{:S(2)}) copy-start(bf16[128,256]{1,0:T(8,128)(2,1)} %param.25) | copy-start | bytes 196612
  2.1 16.0 %copy-start.1 = (bf16[128,2048]{1,0:T(8,128)(2,1)S(1)}, bf16[128,2048]{1,0:T(8,128)(2,1)}, u32[]{:S(2)}) copy-start(bf16[128,2048]{1,0:T(8,128)(2,1)} %param.16) | copy-start | bytes 1572868
  79.8 4.5 %copy-start.10 = (bf16[1024,2048]{1,0:T(8,128)(2,1)S(1)}, bf16[1024,2048]{1,0:T(8,128)(2,1)}, u32[]{:S(2)}) copy-start(bf16[1024,2048]{1,0:T(8,128)(2,1)} %get-tuple-element.15) | copy-start | bytes 12582916
  79.8 4.5 %copy-start.13 = (bf16[1,2048,448]{1,2,0:T(8,128)(2,1)S(1)}, bf16[1,2048,448]{1,2,0:T(8,128)(2,1)}, u32[]{:S(2)}) copy-start(bf16[1,2048,448]{1,2,0:T(8,128)(2,1)} %param.22) | copy-start | bytes 5505028
  84.3 2.2 %copy-start.11 = (bf16[1024,2048]{1,0:T(8,128)(2,1)S(1)}, bf16[1024,2048]{1,0:T(8,128)(2,1)}, u32[]{:S(2)}) copy-start(bf16[1024,2048]{1,0:T(8,128)(2,1)} %get-tuple-element.14) | copy-start | bytes 12582916
  86.5 3.4 %copy-start.12 = (bf16[1,448,2048]{2,1,0:T(8,128)(2,1)S(1)}, bf16[1,448,2048]{2,1,0:T(8,128)(2,1)}, u32[]{:S(2)}) copy-start(bf16[1,448,2048]{2,1,0:T(8,128)(2,1)} %param.23) | copy-start | bytes 5505028
  106.4 50.8 %copy-start.8 = (f32[2048]{0:T(1024)S(1)}, f32[2048]{0:T(1024)}, u32[]{:S(2)}) copy-start(f32[2048]{0:T(1024)} %param.17) | copy-start | bytes 24580
  157.2 3.8 %copy-start.3 = (bf16[2048,256]{1,0:T(8,128)(2,1)S(1)}, bf16[2048,256]{1,0:T(8,128)(2,1)}, u32[]{:S(2)}) copy-start(bf16[2048,256]{1,0:T(8,128)(2,1)} %param.31) | copy-start | bytes 3145732
  158.6 2.9 %copy-start.5 = (f32[128,4,64]{0,2,1:T(8,128)S(1)}, f32[128,4,64]{0,2,1:T(8,128)}, u32[]{:S(2)}) copy-start(f32[128,4,64]{0,2,1:T(8,128)} %get-tuple-element.75) | copy-start | bytes 393220
  160.2 3.5 %copy-start.2 = (bf16[128,2048]{1,0:T(8,128)(2,1)}, bf16[128,2048]{1,0:T(8,128)(2,1)S(1)}, u32[]{:S(2)}) copy-start(bf16[128,2048]{1,0:T(8,128)(2,1)S(1)} %fusion.28.res_ref) | copy-start | bytes 1572868
  160.3 2.1 %copy-start.4 = (f32[1,4,64,64]{3,2,1,0:T(8,128)S(1)}, f32[1,4,64,64]{3,2,1,0:T(8,128)}, u32[]{:S(2)}) copy-start(f32[1,4,64,64]{3,2,1,0:T(8,128)} %param.30) | copy-start | bytes 196612
  198.2 5.5 %copy-start.9 = (f32[32,256]{1,0:T(8,128)S(1)}, f32[32,256]{1,0:T(8,128)}, u32[]{:S(2)}) copy-start(f32[32,256]{1,0:T(8,128)} %get-tuple-element.89) | copy-start | bytes 98308

commit v2 on v0

v2 whole, which is shorter than its diff:
```python
import jax
import jax.numpy as jnp
from jax import lax
from jax.experimental import pallas as pl
from jax.experimental.pallas import tpu as pltpu
from jax.sharding import Mesh
from jax.sharding import PartitionSpec as P

D = 2048
HEADS = 16
STATE = 64
GROUPS = 4
SP = ("sp_0", "sp_1", "sp_2")


EPS = 1e-06
HIGHEST = lax.Precision.HIGHEST


MESH = pl.DeviceIdType.MESH
NZ, NX, NC, NY = 8, 4, 2, 4
NW = NX * NC
CHIPS = NZ * NX
CAP = 16
HALF = CHIPS * CAP
ROWS = 2 * HALF
QUARTER = 512
HID = 448
TOK = 128
CH = 256
HD = 64
LOCAL_HEADS = 4
BF16, F32 = jnp.bfloat16, jnp.float32
CHUNKS = ((0, 0), (0, 1), (1, 0), (1, 1))
WIDE = QUARTER // 2
PIECE = 32
NT = (((1,), (1,)), ((), ()))
TN = (((0,), (0,)), ((), ()))
NN = (((1,), (0,)), ((), ()))


def position():
    return tuple(lax.axis_index(a) for a in ("sp_0", "sp_1", "sp_2", "tp"))


def at(z, x, c, y):
    return {"sp_0": z, "sp_1": x, "sp_2": c, "tp": y}


def remote(src, dst, send, recv, device):
    return pltpu.make_async_remote_copy(
        src_ref=src,
        dst_ref=dst,
        send_sem=send,
        recv_sem=recv,
        device_id=device,
        device_id_type=MESH,
    )


def signal(sem, device):
    pl.semaphore_signal(sem, inc=1, device_id=device, device_id_type=MESH)


def plane_peer(z, x, d):
    return lax.rem(z + d // NX, NZ), lax.rem(x + d % NX, NX)


def greet(z, x, c, y):
    barrier = pltpu.get_barrier_semaphore()

    def hello(d, carry):
        pz, px = plane_peer(z, x, d)
        signal(barrier, at(pz, px, c, y))
        return carry

    lax.fori_loop(1, CHIPS, hello, 0)
    for d in range(NX):
        signal(barrier, at(z, lax.rem(x + d, NX), 1 - c, y))
    signal(barrier, at(z, x, c, lax.rem(y + 1, NY)))
    signal(barrier, at(z, x, c, lax.rem(y + 3, NY)))
    pl.semaphore_wait(barrier, CHIPS - 1 + NX + 2)


def times(n, body):
    def step(i, carry):
        body(i)
        return carry

    lax.fori_loop(0, n, step, 0)


def mult(i, n):
    return pl.multiple_of(i * n, n)


def dot(a, b, dims, precision=None):
    return lax.dot_general(a, b, dims, preferred_element_type=F32, precision=precision)


def layer_kernel(
    in_ref, cot_ref, gated_ref, place_ref, tok_ref, cotan_ref, gain_ref, inv_ref, og_ref, scan_ref,
    growth_ref, read_ref, gw_hbm, uw_hbm, dw_hbm, ow_hbm,
    gg_hbm, ug_hbm, dg_hbm, res_out, opg_out, sg_out, gog_out, later_out,
    rin, rcot, gz, wts, ow, accg, accu, acca, act_t, gp_t, up_t, gp, up_g, wg, po, pm, mate, acc,
    fwd, got, done, back, share_buf, ng, res, msg, box_a, plane, box_b, fan, res_box, prod, opg_box,
    lw, s1, r1, sy, ry, sm, rm, sgz, rgz, spm, rpm, sf, rf, sb, rb, ss, rs, sa, ra, sbb, rbb, sc,
    rc, sr, rr, so, ro,
):
    z, x, c, y = position()
    chip = z * NX + x
    w = x * NC + c
    up, down, far = lax.rem(y + 1, NY), lax.rem(y + 3, NY), lax.rem(y + 2, NY)
    mine, other = c * HALF, (1 - c) * HALF
    part_rows = HALF // 2
    loads = [
        pltpu.make_async_copy(gw_hbm, wts.at[0], lw.at[0]),
        pltpu.make_async_copy(uw_hbm, wts.at[1], lw.at[1]),
        pltpu.make_async_copy(dw_hbm, wts.at[2], lw.at[2]),
        pltpu.make_async_copy(ow_hbm, ow, lw.at[3]),
    ]
    for load in loads:
        load.start()
    sources, targets = (in_ref, cot_ref), (rin, rcot)
    own_rows = pl.ds(pl.multiple_of(chip * CAP, CAP), CAP)
    kept_rows = pl.ds(pl.multiple_of(mine + chip * CAP, CAP), CAP)
    own_cols = pl.ds(mult(y, QUARTER), QUARTER)
    rin[kept_rows, own_cols] = in_ref[own_rows, :]
    rcot[kept_rows, own_cols] = cot_ref[own_rows, :]
    own_tokens = pl.ds(mult(z, TOK), TOK)
    gz[own_tokens, :] = gated_ref[...]
    greet(z, x, c, y)

    def block(k, row, rows, q):
        array, part = CHUNKS[k]
        return targets[array].at[
            pl.ds(pl.multiple_of(row, CAP), rows),
            pl.ds(pl.multiple_of(q * QUARTER + part * WIDE, WIDE), WIDE),
        ]

    short = HALF - CAP

    def issue(k):
        array, part = CHUNKS[k]

        def spread(d, carry):
            pz, px = plane_peer(z, x, d)
            remote(
                sources[array].at[
                    pl.ds(pl.multiple_of((pz * NX + px) * CAP, CAP), CAP), pl.ds(part * WIDE, WIDE)
                ],
                block(k, mine + chip * CAP, CAP, y),
                s1.at[k],
                r1.at[k],
                at(pz, px, c, y),
            ).start()
            return carry

        lax.fori_loop(1, CHIPS, spread, 0)

    def whole(k):
        array, part = CHUNKS[k]
        return remote(
            sources[array].at[pl.ds(0, short), pl.ds(part * WIDE, WIDE)],
            block(k, 0, short, y),
            s1.at[k],
            r1.at[k],
            at(z, x, c, up),
        )

    def relay(k, row, q, slot):
        return remote(
            block(k, row, HALF, q), block(k, row, HALF, q), sm.at[k, slot], rm.at[k, slot],
            at(z, x, 1 - c, y),
        )

    def along(k, row, rows, q, slot, target):
        return remote(
            block(k, row, rows, q), block(k, row, rows, q), sy.at[k, slot], ry.at[k, slot],
            at(z, x, c, target),
        )

    def first(k):
        whole(k).wait_recv()
        along(k, mine, HALF, y, 0, up).start()
        along(k, mine, HALF, y, 1, down).start()
        relay(k, mine, y, 0).start()

    def second(k):
        along(k, mine, HALF, down, 0, up).wait_recv()
        along(k, mine, part_rows, down, 2, up).start()
        relay(k, mine, down, 1).start()
        along(k, mine, HALF, up, 1, down).wait_recv()
        along(k, mine + part_rows, part_rows, up, 3, down).start()
        relay(k, mine, up, 2).start()

    def third(k):
        along(k, mine, part_rows, far, 2, up).wait_recv()
        along(k, mine + part_rows, part_rows, far, 3, down).wait_recv()
        relay(k, mine, far, 3).start()

    def gather(k):
        for slot, q in enumerate((y, down, up, far)):
            relay(k, other, q, slot).wait_recv()

    def forward(k):
        array, part = CHUNKS[k]
        pairs = ((0, accg), (1, accu)) if array == 0 else ((2, acca),)
        rows_ref = targets[array]
        fresh = part == 0

        def body(n):
            nrows = pl.ds(mult(n, 256), 256)
            for index, total in pairs:
                value = None
                for q in range(NY):
                    cols = pl.ds(q * QUARTER + part * WIDE, WIDE)
                    term = dot(wts[index, :, cols], rows_ref[nrows, cols], NT)
                    value = term if value is None else value + term
                if fresh:
                    total[:, nrows] = value
                else:
                    total[:, nrows] += value

        times(ROWS // 256, body)

    def activate():
        def body(i):
            r = pl.ds(mult(i, 16), 16)
            g, u = accg[r, :], accu[r, :]
            s = jax.nn.sigmoid(g)
            silu = g * s
            act_t[r, :] = (silu * u).astype(BF16)
            accu[r, :] = u * s * (1.0 + g * (1.0 - s))
            accg[r, :] = silu

        times(HID // 16, body)

    def grads():
        def body(i):
            r = pl.ds(mult(i, 16), 16)
            a = acca[r, :]
            g = a * accu[r, :]
            u = a * accg[r, :]
            accu[r, :] = g
            accg[r, :] = u
            gp_t[r, :] = g.astype(BF16)
            up_t[r, :] = u.astype(BF16)

        times(HID // 16, body)

        def turn(j):
            cols = pl.ds(mult(j, 128), 128)
            gp[cols, :] = jnp.transpose(accu[:, cols]).astype(BF16)
            up_g[cols, :] = jnp.transpose(accg[:, cols]).astype(BF16)

        times(ROWS // 128, turn)

    issue(0)
    whole(0).wait_send()
    issue(1)
    first(0)
    whole(1).wait_send()
    issue(2)
    first(1)
    second(0)
    whole(2).wait_send()
    issue(3)
    first(2)
    second(1)
    third(0)
    loads[0].wait()
    loads[1].wait()
    gather(0)
    forward(0)
    first(3)
    whole(3).wait_send()

    def line_peer(d):
        p = lax.rem(z + d, NZ)
        return p, at(p, x, c, y)

    def plane_mate(d):
        p = lax.rem(w + d, NW)
        return p, at(z, p // NC, p % NC, y)

    for d in range(1, NZ):
        remote(gated_ref, gz.at[own_tokens, :], sgz, rgz, line_peer(d)[1]).start()
    second(2)
    third(1)
    gather(1)
    forward(1)
    activate()
    second(3)
    third(2)
    loads[2].wait()
    gather(2)
    forward(2)
    third(3)
    gather(3)
    forward(3)
    grads()

    order = (far, up, down, y)

    def product(slot, row, target):
        cols = pl.ds(mult(order[slot], QUARTER), QUARTER)

        def body(i):
            r = pl.ds(pl.multiple_of(row + i * 128, 128), 128)
            value = dot(gp[r, :], wts[0, :, cols], NN) + dot(up_g[r, :], wts[1, :, cols], NN)
            target[slot, pl.ds(mult(i, 128), 128), :] = value.astype(target.dtype)

        times(HALF // 128, body)

    def to_mate(slot):
        return remote(po.at[slot], mate.at[slot], spm.at[slot], rpm.at[slot], at(z, x, 1 - c, y))

    def fold(slot):
        to_mate(slot).wait_recv()

        def body(i):
            r = pl.ds(mult(i, 32), 32)
            acc[slot, r, :] = (pm[slot, r, :] + mate[slot, r, :].astype(F32)).astype(BF16)

        times(HALF // 32, body)

    lo, hi = pl.ds(0, part_rows), pl.ds(part_rows, part_rows)

    def part(ch):
        return pl.ds(ch * WIDE, WIDE)

    def ring(src, dst, slot, ch, target):
        return remote(src, dst, sf.at[slot, ch], rf.at[slot, ch], at(z, x, c, target))

    def f_up(ch):
        return ring(acc.at[0, lo, part(ch)], fwd.at[0, :, part(ch)], 0, ch, up)

    def f_down(ch):
        return ring(acc.at[0, hi, part(ch)], fwd.at[1, :, part(ch)], 1, ch, down)

    def d_up(ch):
        return ring(acc.at[1, hi, part(ch)], got.at[0, hi, part(ch)], 2, ch, up)

    def d_down(ch):
        return ring(acc.at[2, lo, part(ch)], got.at[1, lo, part(ch)], 3, ch, down)

    def a_up(ch):
        return ring(acc.at[1, lo, part(ch)], got.at[0, lo, part(ch)], 4, ch, up)

    def a_down(ch):
        return ring(acc.at[2, hi, part(ch)], got.at[1, hi, part(ch)], 5, ch, down)

    def pass_on(slot, start, index, ch):
        def body(i):
            r = pl.ds(pl.multiple_of(start + i * 32, 32), 32)
            f = pl.ds(mult(i, 32), 32)
            acc[slot, r, part(ch)] = (
                acc[slot, r, part(ch)].astype(F32) + fwd[index, f, part(ch)].astype(F32)
            ).astype(BF16)

        times(part_rows // 32, body)

    def finish(ch):
        def body(i):
            r = pl.ds(mult(i, 32), 32)
            done[r, part(ch)] = (
                acc[3, r, part(ch)].astype(F32)
                + got[0, r, part(ch)].astype(F32)
                + got[1, r, part(ch)].astype(F32)
            ).astype(BF16)

        times(HALF // 32, body)

    def give_back(ch):
        def spread(d, carry):
            pz, px = plane_peer(z, x, d)
            remote(
                done.at[pl.ds(pl.multiple_of((pz * NX + px) * CAP, CAP), CAP), part(ch)],
                back.at[own_rows, part(ch)],
                sb.at[ch],
                rb.at[ch],
                at(pz, px, c, y),
            ).start()
            return carry

        lax.fori_loop(1, CHIPS, spread, 0)
        back[own_rows, part(ch)] = done[own_rows, part(ch)]

    def all_back(ch):
        piece = (pl.ds(0, short), part(ch))
        return remote(done.at[piece], back.at[piece], sb.at[ch], rb.at[ch], at(z, x, c, up))

    def weight_grads(start, stop):
        def step(i, carry):
            cols = pl.ds(mult(i, 256), 256)
            wg[0, :, cols] = dot(gp_t[...], rin[:, cols], NN).astype(BF16)
            wg[1, :, cols] = dot(up_t[...], rin[:, cols], NN).astype(BF16)
            wg[2, :, cols] = dot(act_t[...], rcot[:, cols], NN).astype(BF16)
            return carry

        lax.fori_loop(start, stop, step, 0)

    product(0, other, po)
    to_mate(0).start()
    product(0, mine, pm)
    product(1, other, po)
    to_mate(1).start()
    fold(0)
    f_up(0).start()
    f_down(0).start()
    product(1, mine, pm)
    product(2, other, po)
    to_mate(2).start()
    fold(1)
    d_up(0).start()
    product(2, mine, pm)
    product(3, other, po)
    to_mate(3).start()
    fold(2)
    d_down(0).start()
    f_up(1).start()
    f_down(1).start()
    product(3, mine, pm)
    fold(3)
    f_up(0).wait_recv()
    pass_on(1, 0, 0, 0)
    a_up(0).start()
    f_down(0).wait_recv()
    pass_on(2, part_rows, 1, 0)
    a_down(0).start()
    d_up(1).start()
    d_down(1).start()
    weight_grads(0, 3)
    f_up(1).wait_recv()
    pass_on(1, 0, 0, 1)
    a_up(1).start()
    f_down(1).wait_recv()
    pass_on(2, part_rows, 1, 1)
    a_down(1).start()
    d_up(0).wait_recv()
    d_down(0).wait_recv()
    a_up(0).wait_recv()
    a_down(0).wait_recv()
    finish(0)
    give_back(0)
    weight_grads(3, 6)
    d_up(1).wait_recv()
    d_down(1).wait_recv()
    a_up(1).wait_recv()
    a_down(1).wait_recv()
    finish(1)
    give_back(1)

    first_rows, second_rows = pl.ds(0, TOK // 2), pl.ds(TOK // 2, TOK // 2)
    everything = pl.ds(0, TOK)

    def share(q, piece, slot, target, ch):
        ref = share_buf.at[q, piece, part(ch)]
        return remote(ref, ref, ss.at[slot, ch], rs.at[slot, ch], at(z, x, c, target))

    def place(ch):
        all_back(ch).wait_recv()
        share_buf[y, :, part(ch)] = dot(place_ref[...], back[:, part(ch)], NN).astype(BF16)
        share(y, everything, 0, up, ch).start()
        share(y, everything, 1, down, ch).start()

    def pass_shares(ch):
        share(down, everything, 0, up, ch).wait_recv()
        share(down, first_rows, 2, up, ch).start()
        share(up, everything, 1, down, ch).wait_recv()
        share(up, second_rows, 3, down, ch).start()

    place(0)
    weight_grads(6, 8)
    outs = [
        pltpu.make_async_copy(wg.at[i], hbm, lw.at[4 + i])
        for i, hbm in enumerate((gg_hbm, ug_hbm, dg_hbm))
    ]
    for out in outs:
        out.start()
    pass_shares(0)
    place(1)
    pass_shares(1)
    for ch in range(2):
        share(far, first_rows, 2, up, ch).wait_recv()
        share(far, second_rows, 3, down, ch).wait_recv()

    inv = inv_ref[...]
    dotted = jnp.zeros((TOK, 1), F32)
    for q in range(NY):
        cols = pl.ds(q * QUARTER, QUARTER)
        gained = gain_ref[:, cols] * share_buf[q].astype(F32)
        dotted += jnp.sum(tok_ref[:, cols].astype(F32) * gained, axis=1, keepdims=True)
    coef = inv * inv * inv * dotted / D
    mix = None
    loads[3].wait()
    for q in range(NY):
        cols = pl.ds(q * QUARTER, QUARTER)
        gained = gain_ref[:, cols] * share_buf[q].astype(F32)
        value = (
            cotan_ref[:, cols].astype(F32) + inv * gained - tok_ref[:, cols].astype(F32) * coef
        ).astype(BF16)
        res[:, cols] = value
        term = dot(value, ow[cols, :], NN)
        mix = term if mix is None else mix + term
    res_out[...] = res[:, own_cols]
    res_box[z] = res[:, pl.ds(mult(z, CH), CH)]

    def send_res(d):
        p, device = line_peer(d)
        return remote(
            res.at[:, pl.ds(mult(p, CH), CH)], res_box.at[z], sr.at[d], rr.at[d], device
        )

    def recv_res(d):
        source = lax.rem(z + NZ - d, NZ)
        p, device = line_peer(d)
        return remote(
            res.at[:, pl.ds(mult(p, CH), CH)], res_box.at[source], sr.at[d], rr.at[d], device
        )

    og = og_ref[...].astype(F32)
    sig = jax.nn.sigmoid(og)
    state = mix * og * sig
    sg_out[...] = state
    gog_out[...] = (mix * scan_ref[...] * sig * (1.0 + og * (1.0 - sig))).astype(BF16)
    read = read_ref[...].astype(F32)
    for h in range(LOCAL_HEADS):
        grown = growth_ref[:, h : h + 1] * state[:, h * HD : (h + 1) * HD]
        carried = dot(grown, read, TN, HIGHEST)
        last = growth_ref[TOK - 1 : TOK, h : h + 1]
        for i in range(2):
            msg[2 * h + i, 0:PIECE, :] = carried[i * PIECE : (i + 1) * PIECE, :]
            msg[2 * h + i, PIECE : PIECE + 8, :] = jnp.broadcast_to(last, (8, HD))
    for d in range(1, NW):
        p, device = plane_mate(d)
        remote(msg.at[p], box_a.at[w], sa.at[d], ra.at[d], device).start()
    for d in (1, 7, 2, 6):
        send_res(d).start()
    box_a[w] = msg[w]

    def source_of(d):
        return lax.rem(w + NW - d, NW)

    for d in range(1, NW):
        p, device = plane_mate(d)
        remote(msg.at[p], box_a.at[source_of(d)], sa.at[d], ra.at[d], device).wait_recv()
    data, scale = pl.ds(0, PIECE), pl.ds(PIECE, 8)

    def pair(ref, i):
        s = ref[i, scale, :]
        return ref[i, data, :], jnp.concatenate([s] * (PIECE // 8), axis=0)

    total = jnp.zeros((PIECE, HD), F32)
    decay = jnp.ones((PIECE, HD), F32)
    inside, inside_decay = [], []
    for k in reversed(range(NW)):
        inside.append(total)
        inside_decay.append(decay)
        value, factor = pair(box_a, k)
        total = value + factor * total
        decay = factor * decay
    inside, inside_decay = inside[::-1], inside_decay[::-1]
    plane[data, :] = total
    plane[scale, :] = decay[0:8, :]
    box_b[z, data, :] = total
    box_b[z, scale, :] = decay[0:8, :]
    for d in range(1, NZ):
        remote(plane, box_b.at[z], sbb.at[d], rbb.at[d], line_peer(d)[1]).start()
    for d in (3, 5, 4):
        send_res(d).start()
    for d in range(1, NZ):
        source = lax.rem(z + NZ - d, NZ)
        remote(plane, box_b.at[source], sbb.at[d], rbb.at[d], line_peer(d)[1]).wait_recv()
    beyond = jnp.zeros((PIECE, HD), F32)
    for k in reversed(range(1, NZ)):
        value, factor = pair(box_b, k)
        beyond = jnp.where(k > z, value + factor * beyond, beyond)
    for k in range(NW):
        fan[k] = inside[k] + inside_decay[k] * beyond

    def slot_of(p):
        return later_out.at[p // 2, pl.ds(mult(p % 2, PIECE), PIECE), :]

    for d in range(1, NW):
        p, device = plane_mate(d)
        remote(fan.at[p], slot_of(w), sc.at[d], rc.at[d], device).start()
    later_out[w // 2, pl.ds(mult(w % 2, PIECE), PIECE), :] = fan[w]
    seven = gz.at[pl.ds(0, (NZ - 1) * TOK), :]
    remote(seven, seven, sgz, rgz, at(z, x, c, up)).wait()
    for d in range(1, NZ):
        recv_res(d).wait_recv()
    value = None
    for k in range(NZ):
        term = dot(res_box[k], gz[pl.ds(k * TOK, TOK), :], TN)
        value = term if value is None else value + term
    prod[...] = value.reshape(prod.shape)
    for d in range(1, NW):
        p, device = plane_mate(d)
        remote(prod.at[p], opg_box.at[w], so.at[d], ro.at[d], device).start()
    opg_box[w] = prod[w]
    for d in range(1, NW):
        p, device = plane_mate(d)
        remote(prod.at[p], opg_box.at[source_of(d)], so.at[d], ro.at[d], device).wait_recv()
    opg = opg_box[0]
    for k in range(1, NW):
        opg = opg + opg_box[k]
    opg_out[...] = opg

    for d in range(1, NW):
        p, device = plane_mate(d)
        remote(fan.at[p], slot_of(source_of(d)), sc.at[d], rc.at[d], device).wait_recv()
        remote(msg.at[p], box_a.at[w], sa.at[d], ra.at[d], device).wait_send()
        remote(fan.at[p], slot_of(w), sc.at[d], rc.at[d], device).wait_send()
        remote(prod.at[p], opg_box.at[w], so.at[d], ro.at[d], device).wait_send()
        remote(plane, box_b.at[z], sbb.at[d], rbb.at[d], line_peer(d)[1]).wait_send()
        send_res(d).wait_send()
    for k in range(len(CHUNKS)):
        along(k, mine, HALF, y, 0, up).wait_send()
        along(k, mine, HALF, y, 1, down).wait_send()
        along(k, mine, part_rows, down, 2, up).wait_send()
        along(k, mine + part_rows, part_rows, up, 3, down).wait_send()
        for slot, q in enumerate((y, down, up, far)):
            relay(k, mine, q, slot).wait_send()
    for slot in range(NY):
        to_mate(slot).wait_send()
    for ch in range(2):
        for copy in (f_up, f_down, d_up, d_down, a_up, a_down, all_back):
            copy(ch).wait_send()
        share(y, everything, 0, up, ch).wait_send()
        share(y, everything, 1, down, ch).wait_send()
        share(down, first_rows, 2, up, ch).wait_send()
        share(up, second_rows, 3, down, ch).wait_send()
    for out in outs:
        out.wait()


def layer(*operands):
    dma = pltpu.SemaphoreType.DMA
    vmem, hbm = pl.BlockSpec(memory_space=pltpu.VMEM), pl.BlockSpec(memory_space=pl.ANY)
    n = len(CHUNKS)
    shape = jax.ShapeDtypeStruct
    wide = shape((HID, D), BF16)
    return pl.pallas_call(
        layer_kernel,
        out_shape=(
            wide,
            wide,
            wide,
            shape((TOK, QUARTER), BF16),
            shape((32, CH), F32),
            shape((TOK, CH), F32),
            shape((TOK, CH), BF16),
            shape((LOCAL_HEADS, HD, HD), F32),
        ),
        in_specs=[vmem] * 12 + [hbm] * 4,
        out_specs=(hbm,) * 3 + (vmem,) * 5,
        scratch_shapes=[
            pltpu.VMEM((ROWS, D), BF16),
            pltpu.VMEM((ROWS, D), BF16),
            pltpu.VMEM((NZ * TOK, CH), BF16),
            pltpu.VMEM((3, HID, D), BF16),
            pltpu.VMEM((D, CH), BF16),
            pltpu.VMEM((HID, ROWS), F32),
            pltpu.VMEM((HID, ROWS), F32),
            pltpu.VMEM((HID, ROWS), F32),
            pltpu.VMEM((HID, ROWS), BF16),
            pltpu.VMEM((HID, ROWS), BF16),
            pltpu.VMEM((HID, ROWS), BF16),
            pltpu.VMEM((ROWS, HID), BF16),
            pltpu.VMEM((ROWS, HID), BF16),
            pltpu.VMEM((3, HID, D), BF16),
            pltpu.VMEM((NY, HALF, QUARTER), BF16),
            pltpu.VMEM((NY, HALF, QUARTER), F32),
            pltpu.VMEM((NY, HALF, QUARTER), BF16),
            pltpu.VMEM((NY, HALF, QUARTER), BF16),
            pltpu.VMEM((2, HALF // 2, QUARTER), BF16),
            pltpu.VMEM((2, HALF, QUARTER), BF16),
            pltpu.VMEM((HALF, QUARTER), BF16),
            pltpu.VMEM((HALF, QUARTER), BF16),
            pltpu.VMEM((NY, TOK, QUARTER), BF16),
            pltpu.VMEM((8, 128), F32),
            pltpu.VMEM((TOK, D), BF16),
            pltpu.VMEM((NW, PIECE + 8, HD), F32),
            pltpu.VMEM((NW, PIECE + 8, HD), F32),
            pltpu.VMEM((PIECE + 8, HD), F32),
            pltpu.VMEM((NZ, PIECE + 8, HD), F32),
            pltpu.VMEM((NW, PIECE, HD), F32),
            pltpu.VMEM((NZ, TOK, CH), BF16),
            pltpu.VMEM((NW, 32, CH), F32),
            pltpu.VMEM((NW, 32, CH), F32),
            dma((7,)),
            dma((n,)),
            dma((n,)),
            dma((n, 4)),
            dma((n, 4)),
            dma((n, 4)),
            dma((n, 4)),
            dma,
            dma,
            dma((NY,)),
            dma((NY,)),
            dma((6, 2)),
            dma((6, 2)),
            dma((2,)),
            dma((2,)),
            dma((4, 2)),
            dma((4, 2)),
        ]
        + [dma((8,))] * 10,
        compiler_params=pltpu.CompilerParams(
            collective_id=0, has_side_effects=True, vmem_limit_bytes=62 * 1024 * 1024
        ),
        name="layer",
    )(*operands)


def prepare(scan_rows, step_rows, write_rows, read_rows, decay_rates, per_group):
    length = scan_rows.shape[0]
    head_count = step_rows.shape[0]
    logdec = jnp.cumsum(-decay_rates[:, None] * step_rows, axis=1)
    causal = jnp.arange(length)[:, None] >= jnp.arange(length)[None, :]
    spread = jnp.where(causal[None, :, :], logdec[:, :, None] - logdec[:, None, :], -jnp.inf)
    weights = jnp.exp(spread)
    inputs = (
        scan_rows.astype(jnp.float32).reshape(length, head_count, -1)
        * jnp.transpose(step_rows)[:, :, None]
    )
    write_head = jnp.repeat(
        write_rows.astype(jnp.float32).reshape(length, -1, STATE), per_group, axis=1
    )
    read_head = jnp.repeat(
        read_rows.astype(jnp.float32).reshape(length, -1, STATE), per_group, axis=1
    )
    scores = jnp.einsum("thn,shn->hts", read_head, write_head, precision=HIGHEST) * weights
    return (logdec, weights, inputs, write_head, read_head, scores)


def block_back(
    step_rows,
    logdec,
    weights,
    inputs,
    write_head,
    read_head,
    scores,
    entry_state,
    state_grad,
    later_state,
    per_group,
):
    length, head_count = (inputs.shape[0], inputs.shape[1])
    growth = jnp.transpose(jnp.exp(logdec))
    shrink = jnp.transpose(jnp.exp(logdec[:, -1:] - logdec))
    in_grad = jnp.einsum("hts,thp->shp", scores, state_grad, precision=HIGHEST)
    in_grad = in_grad + shrink[:, :, None] * jnp.einsum(
        "shn,hpn->shp", write_head, later_state, precision=HIGHEST
    )
    scan_grad = (
        (in_grad * jnp.transpose(step_rows)[:, :, None]).reshape(length, -1).astype(jnp.bfloat16)
    )
    pair_terms = jnp.einsum("thp,shp->hts", state_grad, inputs, precision=HIGHEST) * weights
    read_grad = jnp.einsum("hts,shn->thn", pair_terms, write_head, precision=HIGHEST)
    read_grad = read_grad + growth[:, :, None] * jnp.einsum(
        "thp,hpn->thn", state_grad, entry_state, precision=HIGHEST
    )
    write_grad = jnp.einsum("hts,thn->shn", pair_terms, read_head, precision=HIGHEST)
    write_grad = write_grad + shrink[:, :, None] * jnp.einsum(
        "shp,hpn->shn", inputs, later_state, precision=HIGHEST
    )
    group_count = head_count // per_group
    read_total = (
        jnp.sum(read_grad.reshape(length, group_count, per_group, -1), axis=2)
        .reshape(length, -1)
        .astype(jnp.bfloat16)
    )
    write_total = (
        jnp.sum(write_grad.reshape(length, group_count, per_group, -1), axis=2)
        .reshape(length, -1)
        .astype(jnp.bfloat16)
    )
    return (scan_grad, write_total, read_total)


def shards(
    tokens,
    norm_gain,
    cotangent,
    routes,
    route_weight,
    gate_weight,
    up_weight,
    down_weight,
    scan_input,
    out_gate,
    step_size,
    decay_rate,
    write_keys,
    read_keys,
    start_state,
    out_proj,
):
    tok_rows = tokens.shape[0]
    experts_count = CHIPS
    y = lax.axis_index("tp")
    hidden = tokens.astype(jnp.float32)
    inverse = lax.rsqrt(jnp.mean(hidden * hidden, axis=1) + EPS)

    def quarter_of(a):
        return lax.dynamic_slice_in_dim(a, y * QUARTER, QUARTER, a.ndim - 1)

    normed_q = (
        quarter_of(tokens).astype(jnp.float32) * inverse[:, None] * quarter_of(norm_gain)[None, :]
    ).astype(jnp.bfloat16)
    cot_q = quarter_of(cotangent)
    route_flat = routes.reshape(-1)
    member = (route_flat[:, None] == jnp.arange(experts_count, dtype=jnp.int32)[None, :]).astype(
        jnp.int32
    )
    earlier_count = jnp.sum((jnp.cumsum(member, axis=0) - member) * member, axis=1)
    places = (route_flat * CAP + earlier_count).reshape(tok_rows, 2)
    slot_ids = jnp.arange(experts_count * CAP, dtype=jnp.int32)[:, None]
    first_hit = slot_ids == places[None, :, 0]
    second_hit = slot_ids == places[None, :, 1]
    placing = jnp.logical_or(first_hit, second_hit)
    place_matrix = placing.astype(jnp.bfloat16)
    slot_weight = jnp.sum(
        jnp.where(first_hit, route_weight[None, :, 0], 0.0)
        + jnp.where(second_hit, route_weight[None, :, 1], 0.0),
        axis=1,
    )
    send_in = jnp.dot(place_matrix, normed_q, preferred_element_type=jnp.float32).astype(
        jnp.bfloat16
    )
    send_cot = (
        slot_weight[:, None] * jnp.dot(place_matrix, cot_q, preferred_element_type=jnp.float32)
    ).astype(jnp.bfloat16)
    per_group = HEADS // GROUPS
    entry_state = start_state[0]
    logdec, weights, inputs, write_head, read_head, scores = prepare(
        scan_input, step_size, write_keys, read_keys, decay_rate, per_group
    )
    head_count = inputs.shape[1]
    growth = jnp.transpose(jnp.exp(logdec))
    scan_out = jnp.einsum("hts,shp->thp", scores, inputs, precision=HIGHEST)
    scan_out = scan_out + growth[:, :, None] * jnp.einsum(
        "thn,hpn->thp", read_head, entry_state, precision=HIGHEST
    )
    gate_val = out_gate.astype(jnp.float32).reshape(tok_rows, head_count, -1)
    sigmoid_val = jax.nn.sigmoid(gate_val)
    gated = (scan_out * gate_val * sigmoid_val).reshape(tok_rows, -1).astype(jnp.bfloat16)
    (
        gate_grad,
        up_grad,
        down_grad,
        residual_part,
        out_proj_grad,
        state_grad,
        gate_out_grad,
        later_state,
    ) = layer(
        send_in,
        send_cot,
        gated,
        jnp.transpose(place_matrix),
        tokens,
        cotangent,
        norm_gain[None, :],
        inverse[:, None],
        out_gate,
        scan_out.reshape(tok_rows, -1),
        growth,
        read_keys,
        jnp.transpose(gate_weight[0]),
        jnp.transpose(up_weight[0]),
        down_weight[0],
        out_proj,
    )
    state_grad = state_grad.reshape(tok_rows, head_count, -1)
    scan_grad, write_grad, read_grad = block_back(
        step_size,
        logdec,
        weights,
        inputs,
        write_head,
        read_head,
        scores,
        entry_state,
        state_grad,
        later_state,
        per_group,
    )
    return (
        residual_part,
        jnp.transpose(gate_grad)[None],
        jnp.transpose(up_grad)[None],
        down_grad[None],
        out_proj_grad,
        scan_grad,
        gate_out_grad,
        write_grad,
        read_grad,
    )


def solution(mesh):
    finer = Mesh(mesh.devices.reshape(8, 4, 2, mesh.shape["tp"]), ("sp_0", "sp_1", "sp_2", "tp"))
    in_specs = (
        P(SP, None),
        P(),
        P(SP, None),
        P(SP, None),
        P(SP, None),
        P(SP, None, "tp"),
        P(SP, None, "tp"),
        P(SP, "tp", None),
        P(SP, "tp"),
        P(SP, "tp"),
        P("tp", SP),
        P("tp"),
        P(SP, "tp"),
        P(SP, "tp"),
        P(SP, "tp", None, None),
        P(None, "tp"),
    )
    out_specs = (
        P(SP, "tp"),
        P(SP, None, "tp"),
        P(SP, None, "tp"),
        P(SP, "tp", None),
        P(SP, "tp"),
        P(SP, "tp"),
        P(SP, "tp"),
        P(SP, "tp"),
        P(SP, "tp"),
    )
    return jax.shard_map(
        shards, mesh=finer, in_specs=in_specs, out_specs=out_specs, check_vma=False
    )
```

time: 398 us -> 167 us (0.42)
  blocking collectives: 171 us -> 0 us
  Pallas kernels: 0 us -> 134 us
  waiting for transfers between devices: 109 us -> 0 us
  matrix products: 43.6 us -> 10.7 us
  starting transfers between devices: 23 us -> 0 us
  between operations: 15.1 us -> 0.93 us
  other arithmetic: 15.7 us -> 4.07 us
    pallas_call x0 -> x1, Pallas kernels: none -> 134 us  [layer(): pl.pallas_call(layer_kernel, out_shape=(wide, wide, wide, shape((TOK, QUA...]
    all_to_all x1 -> x0, blocking collectives: 107 us -> none  [side_by_side(): lax.all_to_all(both, axis, split_axis=split_dim, concat_axis=concat_dim,...]
    reduce_scatter x1 -> x0, waiting for transfers between devices: 79.3 us -> none  [shards(): lax.psum_scatter(input_part, 'tp', scatter_dimension=1, tiled=True)]
    all_gather x3 -> x0, blocking collectives: 63.3 us -> none  [all_in_one(): both, at, found = (lax.all_gather(jnp.concatenate(lines), axis), 0, {})]
    dot_general x16 -> x4, matrix products: 36.6 us -> 4.95 us  [the longest x1 2.09 us: shards(): jnp.dot(place_matrix, normed_q, preferred_element_type=jnp.float32)]
    all_to_all x3 -> x0, waiting for transfers between devices: 21.8 us -> none  [the longest x1 16.9 us: shards(): lax.all_to_all(input_quarter.reshape(sp_count, capacity, quarter).astype(...]
    all_to_all x3 -> x0, starting transfers between devices: 20.3 us -> none  [the longest x1 10.9 us: shards(): lax.all_to_all(input_quarter.reshape(sp_count, capacity, quarter).astype(...]
    ppermute x2 -> x0, waiting for transfers between devices: 7.59 us -> none  [swapped(): return lax.ppermute(value, axis, pairs)]
  transfers between devices with their start and end apart: 6 -> 0, of which waited for: 5 -> 0; matrix products, arithmetic and copies ran while one was open for 8% -> 0% of each run, Pallas kernels for 0% -> 0%
where the time goes in v2:
time: 167 us
  Pallas kernels  134 us (80%)
  local copies, waits for them, and re-layouts  16.8 us (10%)
  matrix products  10.7 us (6%)
  other arithmetic  4.07 us (2%)
    pallas_call x1, Pallas kernels, layer(): pl.pallas_call(layer_kernel, out_shape=(wide, wide, wide, shape((TOK, QUA...  134 us
    unnamed x37, local copies, waits for them, and re-layouts  10.8 us

profile of v2, /device:TPU:1, one launch (start us, length us, event | category | flops | bytes accessed | tf_op | source)
XLA Modules:
  0.0 166.6 jit_solution(1101907355749536748)
XLA Ops:
  0.7 0.9 copy.90
  1.8 0.6 reduce-window.6
  3.0 0.7 multiply_add_fusion
  3.8 0.8 slice_bitcast_fusion.1
  4.7 2.0 %fusion.cot_ref = bf16[512,512]{1,0:T(8,128)(2,1)} fusion(f32[512]{0:T(512)S(1)} %add_reduce_fusion, bf16[128,2048]{1,0:T(8,128)(2,1)} %cotan_ref.1, s32[]{:T(128)S(6)} %select_n.16, s32[128]{0:T(128)S(1)} %get-tuple-element.75, s32[128]{0:T(128)S(1)} %get-tuple-element.74), kind=kOutput, calls=%fused_computation.1 | convolution fusion | flops 67829760 | bytes 658436 | tf_op jit(solution)/shard_map/dot_general | solution.py:837
  6.7 0.8 dynamic_slice.10
  7.4 1.2 multiply_reduce_fusion
  8.7 2.1 %convolution_convert_fusion.in_ref = bf16[512,512]{1,0:T(8,128)(2,1)} fusion(f32[512]{0:T(512)S(1)} %dynamic_slice.10, f32[128]{0:T(128)S(1)} %get-tuple-element.77, bf16[128,2048]{1,0:T(8,128)(2,1)} %tok_ref.1, s32[]{:T(128)S(6)} %select_n.16, s32[128]{0:T(128)S(1)} %get-tuple-element.75, s32[128]{0:T(128)S(1)} %get-tuple-element.74), kind=kOutput, calls=%fused_computation.2 | convolution fusion | flops 67829760 | bytes 658948 | tf_op jit(solution)/shard_map/dot_general | solution.py:833
  10.8 0.3 reduce_window_sum.28
  11.9 0.6 convolution_multiply_fusion.2
  12.8 0.6 multiply_convert_fusion.2
  13.4 0.8 copy.100.scan_ref
  14.2 0.7 copy.98.gated_ref
  14.9 0.8 fusion.15.place_ref
  15.7 0.7 copy.99.inv_ref
  16.4 0.7 copy.101.read_ref
  17.1 134.1 %layer.1 = (bf16[448,2048]{1,0:T(8,128)(2,1)}, bf16[448,2048]{1,0:T(8,128)(2,1)}, bf16[448,2048]{1,0:T(8,128)(2,1)}, bf16[128,512]{1,0:T(8,128)(2,1)}, f32[32,25...) custom-call(bf16[512,512]{1,0:T(8,128)(2,1)} %convolution_convert_fusion.in_ref, ...), custom_call_target="tpu_custom_call" | custom-call | tf_op jit(solution)/shard_map/layer/pallas_call | solution.py:645
  151.3 1.0 copy.102
  152.4 0.6 convolution_multiply_fusion.1
  153.0 0.4 fusion.9
  153.4 1.2 fusion.12
  154.6 1.3 fusion.8
  155.9 0.9 fusion.11
  157.1 0.4 fusion.10
  157.5 0.7 copy.105
  158.2 0.7 copy.116
  158.9 3.1 %copy.117 = bf16[1,2048,448]{1,2,0:T(8,128)(2,1)} copy(bf16[1,2048,448]{1,2,0:T(8,128)(2,1)} %bitcast.116) | data formatting | bytes 3670016
  161.9 1.2 copy.118
  163.2 0.9 copy-done.1
  164.1 1.2 copy.119
  165.3 0.6 copy.120
  166.0 0.6 copy.121
  (52 shorter events, 2.3 us)
Async XLA Ops:
  0.6 11.0 %copy-start = (f32[1,4,64,64]{3,2,1,0:T(8,128)S(1)}, f32[1,4,64,64]{3,2,1,0:T(8,128)}, u32[]{:S(2)}) copy-start(f32[1,4,64,64]{3,2,1,0:T(8,128)} %param.30) | copy-start | bytes 196612
  0.7 10.1 %copy-start.13 = (f32[4]{0:T(128)S(1)}, f32[4]{0:T(128)}, u32[]{:S(2)}) copy-start(f32[4]{0:T(128)} %param.27) | copy-start | bytes 52
  0.7 10.1 %copy-start.10 = (f32[4,128]{1,0:T(4,128)S(1)}, f32[4,128]{1,0:T(4,128)}, u32[]{:S(2)}) copy-start(f32[4,128]{1,0:T(4,128)} %param.26) | copy-start | bytes 6148
  0.7 10.9 %copy-start.8 = (bf16[128,64]{0,1:T(8,128)(2,1)S(1)}, bf16[128,64]{0,1:T(8,128)(2,1)}, u32[]{:S(2)}) copy-start(bf16[128,64]{0,1:T(8,128)(2,1)} %param.29) | copy-start | bytes 49156
  0.7 11.2 %copy-start.12 = (bf16[128,64]{0,1:T(8,128)(2,1)S(1)}, bf16[128,64]{0,1:T(8,128)(2,1)}, u32[]{:S(2)}) copy-start(bf16[128,64]{0,1:T(8,128)(2,1)} %param.28) | copy-start | bytes 49156
  0.7 11.9 %copy-start.7 = (bf16[128,256]{1,0:T(8,128)(2,1)S(1)}, bf16[128,256]{1,0:T(8,128)(2,1)}, u32[]{:S(2)}) copy-start(bf16[128,256]{1,0:T(8,128)(2,1)} %param.24) | copy-start | bytes 196612
  0.7 12.0 %copy-start.5 = (bf16[128,256]{1,0:T(8,128)(2,1)S(1)}, bf16[128,256]{1,0:T(8,128)(2,1)}, u32[]{:S(2)}) copy-start(bf16[128,256]{1,0:T(8,128)(2,1)} %og_ref.1) | copy-start | bytes 196612
  11.5 5.6 %copy-start.3 = (f32[4,128]{0,1:T(8,128)}, f32[4,128]{0,1:T(8,128)S(1)}, u32[]{:S(2)}) copy-start(f32[4,128]{0,1:T(8,128)S(1)} %copy.95) | copy-start | bytes 6148
  151.3 5.6 %copy-start.4 = (f32[4,64,64]{2,1,0:T(8,128)S(1)}, f32[4,64,64]{2,1,0:T(8,128)}, u32[]{:S(2)}) copy-start(f32[4,64,64]{2,1,0:T(8,128)} %get-tuple-element.23) | copy-start | bytes 196612
  151.3 6.9 %copy-start.6 = (bf16[128,512]{1,0:T(8,128)(2,1)S(1)}, bf16[128,512]{1,0:T(8,128)(2,1)}, u32[]{:S(2)}) copy-start(bf16[128,512]{1,0:T(8,128)(2,1)} %get-tuple-element.89) | copy-start | bytes 393220
  158.9 3.1 %copy-start.2 = (bf16[448,2048]{1,0:T(8,128)(2,1)S(1)}, bf16[448,2048]{1,0:T(8,128)(2,1)}, u32[]{:S(2)}) copy-start(bf16[448,2048]{1,0:T(8,128)(2,1)} %get-tuple-element.19) | copy-start | bytes 5505028
  161.9 2.2 %copy-start.1 = (bf16[448,2048]{1,0:T(8,128)(2,1)S(1)}, bf16[448,2048]{1,0:T(8,128)(2,1)}, u32[]{:S(2)}) copy-start(bf16[448,2048]{1,0:T(8,128)(2,1)} %get-tuple-element.20) | copy-start | bytes 5505028
  164.1 1.2 copy-start.11
  164.1 1.9 %copy-start.9 = (bf16[128,256]{1,0:T(8,128)(2,1)S(1)}, bf16[128,256]{1,0:T(8,128)(2,1)}, u32[]{:S(2)}) copy-start(bf16[128,256]{1,0:T(8,128)(2,1)} %get-tuple-element.95) | copy-start | bytes 196612

commit v3 on v2

v3 whole, which is shorter than its diff:
```python
import jax
import jax.numpy as jnp
from jax import lax
from jax.experimental import pallas as pl
from jax.experimental.pallas import tpu as pltpu
from jax.sharding import Mesh
from jax.sharding import PartitionSpec as P

D = 2048
HEADS = 16
STATE = 64
GROUPS = 4
SP = ("sp_0", "sp_1", "sp_2")


EPS = 1e-06
HIGHEST = lax.Precision.HIGHEST


MESH = pl.DeviceIdType.MESH
NZ, NX, NC, NY = 8, 4, 2, 4
NW = NX * NC
CHIPS = NZ * NX
CAP = 16
HALF = CHIPS * CAP
ROWS = 2 * HALF
QUARTER = 512
HID = 448
TOK = 128
CH = 256
HD = 64
LOCAL_HEADS = 4
BF16, F32 = jnp.bfloat16, jnp.float32
WIDE = QUARTER // 2
DIRECT = 512
RING = (D - DIRECT) // NY
CHUNKS = (
    (0, 0, 128, 0, QUARTER),
    (0, 128, 128, 128, QUARTER),
    (0, 256, 256, 256, QUARTER),
    (1, 0, 256, DIRECT, RING),
    (1, 256, 128, DIRECT + 256, RING),
    (1, RING, 256, 0, 0),
    (1, RING + 256, 256, 256, 0),
)
RINGED = 5
SLICE = TOK // NY
PARTS = ((0, 256), (256, 128), (384, 128))
PIECE = 16
PACK = 128
NT = (((1,), (1,)), ((), ()))
TN = (((0,), (0,)), ((), ()))
NN = (((1,), (0,)), ((), ()))


def position():
    return tuple(lax.axis_index(a) for a in ("sp_0", "sp_1", "sp_2", "tp"))


def at(z, x, c, y):
    return {"sp_0": z, "sp_1": x, "sp_2": c, "tp": y}


def remote(src, dst, send, recv, device):
    return pltpu.make_async_remote_copy(
        src_ref=src,
        dst_ref=dst,
        send_sem=send,
        recv_sem=recv,
        device_id=device,
        device_id_type=MESH,
    )


def signal(sem, device):
    pl.semaphore_signal(sem, inc=1, device_id=device, device_id_type=MESH)


def plane_peer(z, x, d):
    return lax.rem(z + d // NX, NZ), lax.rem(x + d % NX, NX)


def greet(barrier, z, x, c, y):

    def hello(d, carry):
        pz, px = plane_peer(z, x, d)
        signal(barrier, at(pz, px, c, y))
        return carry

    lax.fori_loop(1, CHIPS, hello, 0)
    for d in range(NX):
        signal(barrier, at(z, lax.rem(x + d, NX), 1 - c, y))
    signal(barrier, at(z, x, c, lax.rem(y + 1, NY)))
    signal(barrier, at(z, x, c, lax.rem(y + 3, NY)))


def times(n, body):
    def step(i, carry):
        body(i)
        return carry

    lax.fori_loop(0, n, step, 0)


def mult(i, n):
    return pl.multiple_of(i * n, n)


def dot(a, b, dims, precision=None):
    return lax.dot_general(a, b, dims, preferred_element_type=F32, precision=precision)


def layer_kernel(
    tok_hbm, cotan_hbm, gain_hbm, routes_hbm, route_weight_hbm, og_hbm, scan_in_hbm, step_hbm,
    rate_ref, keys_hbm, reads_hbm, state_hbm, gw_hbm, uw_hbm, dw_hbm, ow_hbm,
    gg_hbm, ug_hbm, dg_hbm, res_hbm, opg_hbm, scan_hbm, gog_hbm, write_hbm, read_hbm,
    sin, scot, slots, rin, rcot, gated, gz, wts, ow, accg, accu, acca, act_t, gp_t, up_t, gp, up_g,
    wg, po, pm, mate, acc, fwd, got, done, back, share_buf, res, msg, box_a, plane, box_b, fan,
    later, res_box, prod, opg_box, pairs_w, scores, heads_u, heads_silu, heads_gate, heads_sg,
    heads_in, cols_t, reads, writes, res_out, opg_out, scan_out, gog_out, write_out, read_out,
    tok_ref, cotan_ref, gain_ref, routes_ref, route_weight_ref, og_ref, scan_ref, step_ref,
    write_ref, read_ref, state_ref, tok_part, cotan_part, gain_part, li, lw, s1, r1, sy, ry, sm, rm, sgz, rgz, spm, rpm, sf, rf, sb, rb, ss, rs, sq, rq, sa, ra, sbb, rbb,
    sc, rc, sr, rr, so, ro,
):
    z, x, c, y = position()
    chip = z * NX + x
    w = x * NC + c
    up, down, far = lax.rem(y + 1, NY), lax.rem(y + 3, NY), lax.rem(y + 2, NY)
    mine, other = c * HALF, (1 - c) * HALF
    part_rows = HALF // 2
    barrier = pltpu.get_barrier_semaphore()
    own_cols = pl.ds(mult(y, QUARTER), QUARTER)
    ring_cols = pl.ds(pl.multiple_of(DIRECT + y * RING, 128), RING)
    staged_inputs = [
        (routes_hbm, routes_ref),
        (route_weight_hbm, route_weight_ref),
        (gain_hbm, gain_ref),
        (tok_hbm, tok_ref),
        (cotan_hbm, cotan_ref),
        (tok_hbm.at[:, own_cols], tok_part),
        (cotan_hbm.at[:, ring_cols], cotan_part),
        (gain_hbm.at[:, own_cols], gain_part),
        (step_hbm, step_ref),
        (keys_hbm, write_ref),
        (reads_hbm, read_ref),
        (scan_in_hbm, scan_ref),
        (og_hbm, og_ref),
        (state_hbm, state_ref),
    ]
    inputs = [
        pltpu.make_async_copy(hbm, ref, li.at[i]) for i, (hbm, ref) in enumerate(staged_inputs)
    ]
    for copy in inputs:
        copy.start()
    early_inputs, late_inputs = inputs[:8], inputs[8:]
    greet(barrier, z, x, c, y)
    for copy in early_inputs:
        copy.wait()
    loads = [
        pltpu.make_async_copy(gw_hbm, wts.at[0], lw.at[0]),
        pltpu.make_async_copy(uw_hbm, wts.at[1], lw.at[1]),
        pltpu.make_async_copy(dw_hbm, wts.at[2], lw.at[2]),
        pltpu.make_async_copy(ow_hbm, ow, lw.at[3]),
    ]
    for load in loads:
        load.start()
    sources, targets = (sin, scot), (rin, rcot)
    own_rows = pl.ds(pl.multiple_of(chip * CAP, CAP), CAP)
    kept_rows = pl.ds(pl.multiple_of(mine + chip * CAP, CAP), CAP)

    squares = jnp.zeros((TOK, 1), F32)
    for q in range(NY):
        value = tok_ref[:, q * QUARTER : (q + 1) * QUARTER].astype(F32)
        squares += jnp.sum(value * value, axis=1, keepdims=True)
    inv = lax.rsqrt(squares / D + EPS)
    earlier = (
        lax.broadcasted_iota(jnp.int32, (TOK, TOK), 0) < lax.broadcasted_iota(jnp.int32, (TOK, TOK), 1)
    ).astype(BF16)
    expert = lax.broadcasted_iota(jnp.int32, (CHIPS, TOK), 0)
    names = [routes_ref[k : k + 1, :] for k in range(2)]
    members = [(expert == name).astype(F32) for name in names]
    counts = dot((members[0] + members[1]).astype(BF16), earlier, NN)
    slot = lax.broadcasted_iota(jnp.int32, (HALF, TOK), 0).astype(F32)
    hits = [
        slot == name.astype(F32) * CAP + jnp.sum(member * counts, axis=0, keepdims=True)
        for name, member in zip(names, members)
    ]
    slots[...] = jnp.logical_or(hits[0], hits[1]).astype(BF16)
    slot_weight = jnp.sum(
        jnp.where(hits[0], route_weight_ref[0:1, :], 0.0)
        + jnp.where(hits[1], route_weight_ref[1:2, :], 0.0),
        axis=1,
        keepdims=True,
    )
    normed = (tok_part[...].astype(F32) * inv * gain_part[...]).astype(BF16)
    sin[...] = dot(slots[...], normed, NN).astype(BF16)
    scot[:, 0:RING] = (slot_weight * dot(slots[...], cotan_part[...], NN)).astype(BF16)
    scot[:, RING:] = (slot_weight * dot(slots[...], cotan_ref[:, 0:DIRECT], NN)).astype(BF16)
    rin[kept_rows, own_cols] = sin[own_rows, :]
    rcot[kept_rows, ring_cols] = scot[own_rows, 0:RING]
    rcot[kept_rows, 0:DIRECT] = scot[own_rows, RING:]
    pl.semaphore_wait(barrier, CHIPS - 1 + NX + 2)

    def block(k, row, rows, q):
        array, _, width, base, stride = CHUNKS[k]
        return targets[array].at[
            pl.ds(pl.multiple_of(row, CAP), rows),
            pl.ds(pl.multiple_of(base + q * stride, 128), width),
        ]

    short = HALF - CAP

    def staged(k, rows):
        array, column, width, _, _ = CHUNKS[k]
        return sources[array].at[rows, pl.ds(column, width)]

    def issue(k):
        def spread(d, carry):
            pz, px = plane_peer(z, x, d)
            remote(
                staged(k, pl.ds(pl.multiple_of((pz * NX + px) * CAP, CAP), CAP)),
                block(k, mine + chip * CAP, CAP, y),
                s1.at[k],
                r1.at[k],
                at(pz, px, c, y),
            ).start()
            return carry

        lax.fori_loop(1, CHIPS, spread, 0)

    def whole(k):
        return remote(
            staged(k, pl.ds(0, short)), block(k, 0, short, y), s1.at[k], r1.at[k], at(z, x, c, up)
        )

    def relay(k, row, q, slot):
        return remote(
            block(k, row, HALF, q), block(k, row, HALF, q), sm.at[k, slot], rm.at[k, slot],
            at(z, x, 1 - c, y),
        )

    def along(k, row, rows, q, slot, target):
        return remote(
            block(k, row, rows, q), block(k, row, rows, q), sy.at[k, slot], ry.at[k, slot],
            at(z, x, c, target),
        )

    def first(k):
        whole(k).wait_recv()
        along(k, mine, HALF, y, 0, up).start()
        along(k, mine, HALF, y, 1, down).start()
        relay(k, mine, y, 0).start()

    def second(k):
        along(k, mine, HALF, down, 0, up).wait_recv()
        along(k, mine, part_rows, down, 2, up).start()
        relay(k, mine, down, 1).start()
        along(k, mine, HALF, up, 1, down).wait_recv()
        along(k, mine + part_rows, part_rows, up, 3, down).start()
        relay(k, mine, up, 2).start()

    def third(k):
        along(k, mine, part_rows, far, 2, up).wait_recv()
        along(k, mine + part_rows, part_rows, far, 3, down).wait_recv()
        relay(k, mine, far, 3).start()

    def straight(k):
        whole(k).wait_recv()
        relay(k, mine, 0, 0).start()

    def gather(k):
        for slot, q in enumerate((y, down, up, far)):
            if slot == 0 or k < RINGED:
                relay(k, other, q, slot).wait_recv()

    def forward(array, columns, width, fresh):
        pairs = ((0, accg), (1, accu)) if array == 0 else ((2, acca),)
        rows_ref = targets[array]

        def body(n):
            nrows = pl.ds(mult(n, 256), 256)
            for index, total in pairs:
                value = None
                for group in columns:
                    left = [wts[index, :, column : column + width] for column in group]
                    right = [rows_ref[nrows, column : column + width] for column in group]
                    if len(group) > 1:
                        left = [jnp.concatenate(left, axis=1)]
                        right = [jnp.concatenate(right, axis=1)]
                    term = dot(left[0], right[0], NT)
                    value = term if value is None else value + term
                if fresh:
                    total[:, nrows] = value
                else:
                    total[:, nrows] += value

        times(ROWS // 256, body)

    def activate():
        def body(i):
            r = pl.ds(mult(i, 16), 16)
            g, u = accg[r, :], accu[r, :]
            s = jax.nn.sigmoid(g)
            silu = g * s
            act_t[r, :] = (silu * u).astype(BF16)
            accu[r, :] = u * s * (1.0 + g * (1.0 - s))
            accg[r, :] = silu

        times(HID // 16, body)

    def grads():
        def body(i):
            r = pl.ds(mult(i, 16), 16)
            a = acca[r, :]
            g = a * accu[r, :]
            u = a * accg[r, :]
            accu[r, :] = g
            accg[r, :] = u
            gp_t[r, :] = g.astype(BF16)
            up_t[r, :] = u.astype(BF16)

        times(HID // 16, body)

        def turn(j):
            cols = pl.ds(mult(j, 128), 128)
            gp[cols, :] = jnp.transpose(accu[:, cols]).astype(BF16)
            up_g[cols, :] = jnp.transpose(accg[:, cols]).astype(BF16)

        times(ROWS // 128, turn)

    def prepare():
        reads[...] = jnp.transpose(read_ref[...].astype(F32))
        writes[...] = jnp.transpose(write_ref[...].astype(F32))
        upto = (
            lax.broadcasted_iota(jnp.int32, (TOK, TOK), 0)
            <= lax.broadcasted_iota(jnp.int32, (TOK, TOK), 1)
        ).astype(F32)
        delta = jnp.concatenate(
            [-rate_ref[h] * step_ref[h : h + 1, :] for h in range(LOCAL_HEADS)], axis=0
        )
        logdec = dot(delta, upto, NN, HIGHEST)
        columns = jnp.transpose(jnp.concatenate([logdec, step_ref[...]], axis=0))
        cols_t[...] = columns
        causal = lax.broadcasted_iota(jnp.int32, (TOK, TOK), 0) >= lax.broadcasted_iota(
            jnp.int32, (TOK, TOK), 1
        )
        keys = dot(read_ref[...], write_ref[...], TN)
        for h in range(LOCAL_HEADS):
            spread = jnp.where(causal, columns[:, h : h + 1] - logdec[h : h + 1, :], -jnp.inf)
            weights = jnp.exp(spread)
            pairs_w[h] = weights
            scores[h] = keys * weights

    def scan_head(h):
        lanes = slice(h * HD, (h + 1) * HD)
        u = scan_ref[:, lanes].astype(F32) * cols_t[:, LOCAL_HEADS + h : LOCAL_HEADS + h + 1]
        heads_u[h] = u
        value = dot(scores[h], u, NN, HIGHEST)
        value += jnp.exp(cols_t[:, h : h + 1]) * dot(reads[...], state_ref[h], NT, HIGHEST)
        og = og_ref[:, lanes].astype(F32)
        sig = jax.nn.sigmoid(og)
        gated[:, lanes] = (value * og * sig).astype(BF16)
        heads_silu[h] = og * sig
        heads_gate[h] = value * sig * (1.0 + og * (1.0 - sig))

    def line_peer(d):
        p = lax.rem(z + d, NZ)
        return p, at(p, x, c, y)

    def plane_mate(d):
        p = lax.rem(w + d, NW)
        return p, at(z, p // NC, p % NC, y)

    own_tokens = pl.ds(mult(z, TOK), TOK)
    ring_in = [(q * QUARTER,) for q in range(NY)]
    next_in = [(q * QUARTER + 256,) for q in range(NY)]
    ring_cot = [(DIRECT + q * RING,) for q in range(NY)]
    last_cot = [tuple(DIRECT + q * RING + 256 for q in pair) for pair in ((0, 1), (2, 3))]
    issue(0)
    for copy in late_inputs:
        copy.wait()
    prepare()
    whole(0).wait_send()
    issue(1)
    scan_head(0)
    first(0)
    whole(1).wait_send()
    issue(2)
    scan_head(1)
    first(1)
    scan_head(2)
    second(0)
    whole(2).wait_send()
    issue(3)
    scan_head(3)
    gz[own_tokens, :] = gated[...]
    second(1)
    first(2)
    whole(3).wait_send()
    issue(4)
    third(0)
    third(1)
    first(3)
    whole(4).wait_send()
    issue(5)
    loads[0].wait()
    loads[1].wait()
    second(2)
    first(4)
    gather(0)
    gather(1)
    forward(0, ring_in, 256, True)
    whole(5).wait_send()
    issue(6)
    second(3)
    for d in range(1, NZ):
        remote(gated, gz.at[own_tokens, :], sgz, rgz, line_peer(d)[1]).start()
    straight(5)
    third(2)
    gather(2)
    forward(0, next_in, 256, False)
    second(4)
    activate()
    straight(6)
    third(3)
    loads[2].wait()
    gather(3)
    forward(1, ring_cot, 256, True)
    gather(5)
    gather(6)
    forward(1, [(0,)], DIRECT, False)
    third(4)
    gather(4)
    forward(1, last_cot, 128, False)
    grads()

    order = (far, up, down, y)

    def product(slot, row, target):
        cols = pl.ds(mult(order[slot], QUARTER), QUARTER)

        def body(i):
            r = pl.ds(pl.multiple_of(row + i * 256, 256), 256)
            value = dot(gp[r, :], wts[0, :, cols], NN) + dot(up_g[r, :], wts[1, :, cols], NN)
            target[slot, pl.ds(mult(i, 256), 256), :] = value.astype(target.dtype)

        times(HALF // 256, body)

    def to_mate(slot):
        return remote(po.at[slot], mate.at[slot], spm.at[slot], rpm.at[slot], at(z, x, 1 - c, y))

    def fold(slot):
        to_mate(slot).wait_recv()

        def body(i):
            r = pl.ds(mult(i, 32), 32)
            acc[slot, r, :] = (pm[slot, r, :] + mate[slot, r, :].astype(F32)).astype(BF16)

        times(HALF // 32, body)

    lo, hi = pl.ds(0, part_rows), pl.ds(part_rows, part_rows)

    def part(ch):
        return pl.ds(*PARTS[ch])

    def ring(src, dst, slot, ch, target):
        return remote(src, dst, sf.at[slot, ch], rf.at[slot, ch], at(z, x, c, target))

    def f_up(ch):
        return ring(acc.at[0, lo, part(ch)], fwd.at[0, :, part(ch)], 0, ch, up)

    def f_down(ch):
        return ring(acc.at[0, hi, part(ch)], fwd.at[1, :, part(ch)], 1, ch, down)

    def d_up(ch):
        return ring(acc.at[1, hi, part(ch)], got.at[0, hi, part(ch)], 2, ch, up)

    def d_down(ch):
        return ring(acc.at[2, lo, part(ch)], got.at[1, lo, part(ch)], 3, ch, down)

    def a_up(ch):
        return ring(acc.at[1, lo, part(ch)], got.at[0, lo, part(ch)], 4, ch, up)

    def a_down(ch):
        return ring(acc.at[2, hi, part(ch)], got.at[1, hi, part(ch)], 5, ch, down)

    def pass_on(slot, start, index, ch):
        def body(i):
            r = pl.ds(pl.multiple_of(start + i * 32, 32), 32)
            f = pl.ds(mult(i, 32), 32)
            acc[slot, r, part(ch)] = (
                acc[slot, r, part(ch)].astype(F32) + fwd[index, f, part(ch)].astype(F32)
            ).astype(BF16)

        times(part_rows // 32, body)

    def finish(ch):
        def body(i):
            r = pl.ds(mult(i, 32), 32)
            done[r, part(ch)] = (
                acc[3, r, part(ch)].astype(F32)
                + got[0, r, part(ch)].astype(F32)
                + got[1, r, part(ch)].astype(F32)
            ).astype(BF16)

        times(HALF // 32, body)

    def give_back(ch):
        def spread(d, carry):
            pz, px = plane_peer(z, x, d)
            remote(
                done.at[pl.ds(pl.multiple_of((pz * NX + px) * CAP, CAP), CAP), part(ch)],
                back.at[own_rows, part(ch)],
                sb.at[ch],
                rb.at[ch],
                at(pz, px, c, y),
            ).start()
            return carry

        lax.fori_loop(1, CHIPS, spread, 0)
        back[own_rows, part(ch)] = done[own_rows, part(ch)]

    def all_back(ch):
        piece = (pl.ds(0, short), part(ch))
        return remote(done.at[piece], back.at[piece], sb.at[ch], rb.at[ch], at(z, x, c, up))

    def weight_grads(start, stop):
        def step(i, carry):
            cols = pl.ds(mult(i, 256), 256)
            wg[0, :, cols] = dot(gp_t[...], rin[:, cols], NN).astype(BF16)
            wg[1, :, cols] = dot(up_t[...], rin[:, cols], NN).astype(BF16)
            wg[2, :, cols] = dot(act_t[...], rcot[:, cols], NN).astype(BF16)
            return carry

        lax.fori_loop(start, stop, step, 0)

    product(0, other, po)
    to_mate(0).start()
    product(0, mine, pm)
    product(1, other, po)
    to_mate(1).start()
    fold(0)
    f_up(0).start()
    f_down(0).start()
    product(1, mine, pm)
    product(2, other, po)
    to_mate(2).start()
    fold(1)
    d_up(0).start()
    product(2, mine, pm)
    product(3, other, po)
    to_mate(3).start()
    fold(2)
    d_down(0).start()

    def turn(ch):
        f_up(ch).wait_recv()
        pass_on(1, 0, 0, ch)
        a_up(ch).start()
        f_down(ch).wait_recv()
        pass_on(2, part_rows, 1, ch)
        a_down(ch).start()

    def launch(ch):
        f_up(ch).start()
        f_down(ch).start()
        d_up(ch).start()
        d_down(ch).start()

    def complete(ch):
        d_up(ch).wait_recv()
        d_down(ch).wait_recv()
        a_up(ch).wait_recv()
        a_down(ch).wait_recv()
        finish(ch)
        give_back(ch)

    turn(0)
    launch(1)
    product(3, mine, pm)
    fold(3)
    weight_grads(0, 2)
    turn(1)
    launch(2)
    weight_grads(2, 3)
    complete(0)
    turn(2)
    weight_grads(3, 5)
    complete(1)
    weight_grads(5, 6)
    complete(2)

    first_rows, second_rows = pl.ds(0, TOK // 2), pl.ds(TOK // 2, TOK // 2)
    everything = pl.ds(0, TOK)

    def share(q, piece, slot, target, ch):
        ref = share_buf.at[q, piece, part(ch)]
        return remote(ref, ref, ss.at[slot, ch], rs.at[slot, ch], at(z, x, c, target))

    def place(ch):
        all_back(ch).wait_recv()
        share_buf[y, :, part(ch)] = dot(slots[...], back[:, part(ch)], TN).astype(BF16)
        share(y, everything, 0, up, ch).start()
        share(y, everything, 1, down, ch).start()

    def pass_shares(ch):
        share(down, everything, 0, up, ch).wait_recv()
        share(down, first_rows, 2, up, ch).start()
        share(up, everything, 1, down, ch).wait_recv()
        share(up, second_rows, 3, down, ch).start()

    def sent_dispatch():
        for k in range(RINGED):
            along(k, mine, HALF, y, 0, up).wait_send()
            along(k, mine, HALF, y, 1, down).wait_send()
            along(k, mine, part_rows, down, 2, up).wait_send()
            along(k, mine + part_rows, part_rows, up, 3, down).wait_send()
            for slot, q in enumerate((y, down, up, far)):
                relay(k, mine, q, slot).wait_send()
        whole(6).wait_send()
        for k in range(RINGED, len(CHUNKS)):
            relay(k, mine, 0, 0).wait_send()

    def sent_ring():
        for slot in range(NY):
            to_mate(slot).wait_send()
        for ch in range(len(PARTS)):
            for copy in (f_up, f_down, d_up, d_down, a_up, a_down, all_back):
                copy(ch).wait_send()
            share(y, everything, 0, up, ch).wait_send()
            share(y, everything, 1, down, ch).wait_send()
            share(down, first_rows, 2, up, ch).wait_send()
            share(up, second_rows, 3, down, ch).wait_send()

    def sent_carry():
        for d in range(1, NW):
            p, device = plane_mate(d)
            remote(msg.at[p], box_a.at[w], sa.at[d], ra.at[d], device).wait_send()
            remote(plane, box_b.at[z], sbb.at[d], rbb.at[d], line_peer(d)[1]).wait_send()
            send_res(d, z).wait_send()
        ring_res(y, every, 0, up).wait_send()
        ring_res(y, every, 1, down).wait_send()

    place(0)
    weight_grads(6, 8)
    outs = [
        pltpu.make_async_copy(wg.at[i], hbm, lw.at[4 + i])
        for i, hbm in enumerate((gg_hbm, ug_hbm, dg_hbm))
    ]
    for out in outs:
        out.start()

    def put(ref, hbm):
        copy = pltpu.make_async_copy(ref, hbm, lw.at[4 + len(outs)])
        copy.start()
        outs.append(copy)

    place(1)
    pass_shares(0)
    place(2)
    pass_shares(1)
    pass_shares(2)
    dotted = jnp.zeros((TOK, 1), F32)

    def dotted_with(q):
        cols = pl.ds(mult(q, QUARTER), QUARTER)
        gained = gain_ref[:, cols] * share_buf[q].astype(F32)
        return jnp.sum(tok_ref[:, cols].astype(F32) * gained, axis=1, keepdims=True)

    loads[3].wait()
    sent_dispatch()
    dotted += dotted_with(y) + dotted_with(down) + dotted_with(up)
    for ch in range(len(PARTS)):
        share(far, first_rows, 2, up, ch).wait_recv()
        share(far, second_rows, 3, down, ch).wait_recv()

    dotted += dotted_with(far)
    coef = inv * inv * inv * dotted / D
    mix = None
    for q in range(NY):
        cols = pl.ds(q * QUARTER, QUARTER)
        gained = gain_ref[:, cols] * share_buf[q].astype(F32)
        value = (
            cotan_ref[:, cols].astype(F32) + inv * gained - tok_ref[:, cols].astype(F32) * coef
        ).astype(BF16)
        res[:, cols] = value
        term = dot(value, ow[cols, :], NN)
        mix = term if mix is None else mix + term
    res_out[...] = res[:, own_cols]
    put(res_out, res_hbm)
    slice_rows = pl.ds(mult(y, SLICE), SLICE)

    def boxed(source):
        return res_box.at[y, pl.ds(mult(source, SLICE), SLICE), :]

    res_box[y, pl.ds(mult(z, SLICE), SLICE), :] = res[slice_rows, pl.ds(mult(z, CH), CH)]

    def send_res(d, source):
        p, device = line_peer(d)
        return remote(
            res.at[slice_rows, pl.ds(mult(p, CH), CH)], boxed(source), sr.at[d], rr.at[d], device
        )

    for d in range(1, NZ):
        send_res(d, z).start()
    read, write = reads[...], writes[...]
    for h in range(LOCAL_HEADS):
        lanes = slice(h * HD, (h + 1) * HD)
        sg = mix[:, lanes] * heads_silu[h]
        heads_sg[h] = sg
        growth = jnp.exp(cols_t[:, h : h + 1])
        carried = dot(growth * sg, read, TN, HIGHEST)
        for i in range(2):
            start = 2 * i * PIECE
            msg[2 * h + i, 0:PIECE, :] = jnp.concatenate(
                [carried[start : start + PIECE, :], carried[start + PIECE : start + 2 * PIECE, :]],
                axis=1,
            )
            msg[2 * h + i, PIECE : PIECE + 8, :] = jnp.broadcast_to(
                growth[TOK - 1 :, :], (8, PACK)
            )
    for d in range(1, NW):
        p, device = plane_mate(d)
        remote(msg.at[p], box_a.at[w], sa.at[d], ra.at[d], device).start()
    box_a[w] = msg[w]
    read_grads, write_grads = [], []

    def head_back(h):
        lanes = slice(h * HD, (h + 1) * HD)
        sg = heads_sg[h]
        gog_out[:, lanes] = (mix[:, lanes] * heads_gate[h]).astype(BF16)
        heads_in[h] = dot(scores[h], sg, TN, HIGHEST)
        pair_terms = dot(sg, heads_u[h], NT, HIGHEST) * pairs_w[h]
        read_grads.append(
            dot(pair_terms, write, NN, HIGHEST)
            + jnp.exp(cols_t[:, h : h + 1]) * dot(sg, state_ref[h], NN, HIGHEST)
        )
        write_grads.append(dot(pair_terms, read, TN, HIGHEST))

    head_back(0)
    head_back(1)

    def source_of(d):
        return lax.rem(w + NW - d, NW)

    for d in range(1, NW):
        p, device = plane_mate(d)
        remote(msg.at[p], box_a.at[source_of(d)], sa.at[d], ra.at[d], device).wait_recv()
    data, scale = pl.ds(0, PIECE), pl.ds(PIECE, 8)

    def pair(ref, i):
        s = ref[i, scale, :]
        return ref[i, data, :], jnp.concatenate([s] * (PIECE // 8), axis=0)

    total = jnp.zeros((PIECE, PACK), F32)
    decay = jnp.ones((PIECE, PACK), F32)
    inside, inside_decay = [], []
    for k in reversed(range(NW)):
        inside.append(total)
        inside_decay.append(decay)
        value, factor = pair(box_a, k)
        total = value + factor * total
        decay = factor * decay
    inside, inside_decay = inside[::-1], inside_decay[::-1]
    plane[data, :] = total
    plane[scale, :] = decay[0:8, :]
    box_b[z, data, :] = total
    box_b[z, scale, :] = decay[0:8, :]
    for d in range(1, NZ):
        remote(plane, box_b.at[z], sbb.at[d], rbb.at[d], line_peer(d)[1]).start()
    for d in range(1, NZ):
        send_res(d, lax.rem(z + NZ - d, NZ)).wait_recv()

    def ring_res(q, rows, slot, target):
        ref = res_box.at[q, rows, :]
        return remote(ref, ref, sq.at[slot], rq.at[slot], at(z, x, c, target))

    every, early, late = (
        pl.ds(0, NZ * SLICE),
        pl.ds(0, NZ * SLICE // 2),
        pl.ds(NZ * SLICE // 2, NZ * SLICE // 2),
    )
    ring_res(y, every, 0, up).start()
    ring_res(y, every, 1, down).start()
    head_back(2)
    for d in range(1, NZ):
        source = lax.rem(z + NZ - d, NZ)
        remote(plane, box_b.at[source], sbb.at[d], rbb.at[d], line_peer(d)[1]).wait_recv()
    beyond = jnp.zeros((PIECE, PACK), F32)
    for k in reversed(range(1, NZ)):
        value, factor = pair(box_b, k)
        beyond = jnp.where(k > z, value + factor * beyond, beyond)
    for k in range(NW):
        fan[k] = inside[k] + inside_decay[k] * beyond

    def slot_of(p):
        return later.at[p]

    for d in range(1, NW):
        p, device = plane_mate(d)
        remote(fan.at[p], slot_of(w), sc.at[d], rc.at[d], device).start()
    later[w] = fan[w]
    head_back(3)
    put(gog_out, gog_hbm)
    sent_ring()
    ring_res(down, every, 0, up).wait_recv()
    ring_res(down, early, 2, up).start()
    ring_res(up, every, 1, down).wait_recv()
    ring_res(up, late, 3, down).start()
    seven = gz.at[pl.ds(0, (NZ - 1) * TOK), :]
    remote(seven, seven, sgz, rgz, at(z, x, c, up)).wait()
    for d in range(1, NW):
        p, device = plane_mate(d)
        remote(fan.at[p], slot_of(source_of(d)), sc.at[d], rc.at[d], device).wait_recv()

    def head_end(h):
        lanes = slice(h * HD, (h + 1) * HD)
        column = cols_t[:, h : h + 1]
        shrink = jnp.exp(column[TOK - 1 :, :] - column)
        state = jnp.concatenate(
            [later[2 * h + i, :, j * HD : (j + 1) * HD] for i in range(2) for j in range(2)], axis=0
        )
        value = heads_in[h] + shrink * dot(write, state, NT, HIGHEST)
        scan_out[:, lanes] = (value * cols_t[:, LOCAL_HEADS + h : LOCAL_HEADS + h + 1]).astype(BF16)
        write_grads[h] += shrink * dot(heads_u[h], state, NN, HIGHEST)

    for h in range(LOCAL_HEADS):
        head_end(h)
    put(scan_out, scan_hbm)
    ring_res(far, early, 2, up).wait_recv()
    ring_res(far, late, 3, down).wait_recv()
    value = None
    for q in range(NY):
        rows = jnp.concatenate(
            [gz[k * TOK + q * SLICE : k * TOK + (q + 1) * SLICE, :] for k in range(NZ)], axis=0
        )
        term = dot(res_box[q], rows, TN)
        value = term if value is None else value + term
    prod[...] = value.reshape(prod.shape).astype(BF16)
    for d in range(1, NW):
        p, device = plane_mate(d)
        remote(prod.at[p], opg_box.at[w], so.at[d], ro.at[d], device).start()
    opg_box[w] = prod[w]
    write_out[...] = jnp.transpose(sum(write_grads[1:], write_grads[0])).astype(BF16)
    read_out[...] = jnp.transpose(sum(read_grads[1:], read_grads[0])).astype(BF16)
    put(write_out, write_hbm)
    put(read_out, read_hbm)
    sent_carry()
    for d in range(1, NW):
        p, device = plane_mate(d)
        remote(prod.at[p], opg_box.at[source_of(d)], so.at[d], ro.at[d], device).wait_recv()
    opg = opg_box[0].astype(F32)
    for k in range(1, NW):
        opg = opg + opg_box[k].astype(F32)
    opg_out[...] = opg
    put(opg_out, opg_hbm)

    for d in range(1, NW):
        p, device = plane_mate(d)
        remote(fan.at[p], slot_of(w), sc.at[d], rc.at[d], device).wait_send()
        remote(prod.at[p], opg_box.at[w], so.at[d], ro.at[d], device).wait_send()
    ring_res(down, early, 2, up).wait_send()
    ring_res(up, late, 3, down).wait_send()
    for out in outs:
        out.wait()


def layer(*operands):
    dma = pltpu.SemaphoreType.DMA
    hbm = pl.BlockSpec(memory_space=pl.ANY)
    smem = pl.BlockSpec(memory_space=pltpu.SMEM)
    n = len(CHUNKS)
    shape = jax.ShapeDtypeStruct
    wide = shape((HID, D), BF16)

    def held(*dims, dtype=BF16):
        return pltpu.VMEM(dims, dtype)

    head = held(LOCAL_HEADS, TOK, HD, dtype=F32)
    return pl.pallas_call(
        layer_kernel,
        out_shape=(
            wide,
            wide,
            wide,
            shape((TOK, QUARTER), BF16),
            shape((32, CH), F32),
            shape((TOK, CH), BF16),
            shape((TOK, CH), BF16),
            shape((HD, TOK), BF16),
            shape((HD, TOK), BF16),
        ),
        in_specs=[hbm] * 8 + [smem] + [hbm] * 7,
        out_specs=(hbm,) * 9,
        scratch_shapes=[
            held(HALF, QUARTER),
            held(HALF, RING + DIRECT),
            held(HALF, TOK),
            held(ROWS, D),
            held(ROWS, D),
            held(TOK, CH),
            held(NZ * TOK, CH),
            held(3, HID, D),
            held(D, CH),
            held(HID, ROWS, dtype=F32),
            held(HID, ROWS, dtype=F32),
            held(HID, ROWS, dtype=F32),
            held(HID, ROWS),
            held(HID, ROWS),
            held(HID, ROWS),
            held(ROWS, HID),
            held(ROWS, HID),
            held(3, HID, D),
            held(NY, HALF, QUARTER),
            held(NY, HALF, QUARTER, dtype=F32),
            held(NY, HALF, QUARTER),
            held(NY, HALF, QUARTER),
            held(2, HALF // 2, QUARTER),
            held(2, HALF, QUARTER),
            held(HALF, QUARTER),
            held(HALF, QUARTER),
            held(NY, TOK, QUARTER),
            held(TOK, D),
            held(NW, PIECE + 8, PACK, dtype=F32),
            held(NW, PIECE + 8, PACK, dtype=F32),
            held(PIECE + 8, PACK, dtype=F32),
            held(NZ, PIECE + 8, PACK, dtype=F32),
            held(NW, PIECE, PACK, dtype=F32),
            held(NW, PIECE, PACK, dtype=F32),
            held(NY, NZ * SLICE, CH),
            held(NW, 32, CH),
            held(NW, 32, CH),
            held(LOCAL_HEADS, TOK, TOK, dtype=F32),
            held(LOCAL_HEADS, TOK, TOK, dtype=F32),
            head,
            head,
            head,
            head,
            head,
            held(TOK, 2 * LOCAL_HEADS, dtype=F32),
            held(TOK, HD, dtype=F32),
            held(TOK, HD, dtype=F32),
            held(TOK, QUARTER),
            held(32, CH, dtype=F32),
            held(TOK, CH),
            held(TOK, CH),
            held(HD, TOK),
            held(HD, TOK),
            held(TOK, D),
            held(TOK, D),
            held(1, D, dtype=F32),
            held(2, TOK, dtype=jnp.int32),
            held(2, TOK, dtype=F32),
            held(TOK, CH),
            held(TOK, CH),
            held(LOCAL_HEADS, TOK, dtype=F32),
            held(HD, TOK),
            held(HD, TOK),
            held(LOCAL_HEADS, HD, HD, dtype=F32),
            held(TOK, QUARTER),
            held(TOK, RING),
            held(1, QUARTER, dtype=F32),
            dma((14,)),
            dma((13,)),
            dma((n,)),
            dma((n,)),
            dma((n, 4)),
            dma((n, 4)),
            dma((n, 4)),
            dma((n, 4)),
            dma,
            dma,
            dma((NY,)),
            dma((NY,)),
            dma((6, len(PARTS))),
            dma((6, len(PARTS))),
            dma((len(PARTS),)),
            dma((len(PARTS),)),
            dma((4, len(PARTS))),
            dma((4, len(PARTS))),
            dma((4,)),
            dma((4,)),
        ]
        + [dma((8,))] * 10,
        compiler_params=pltpu.CompilerParams(
            collective_id=0, has_side_effects=True, vmem_limit_bytes=62 * 1024 * 1024
        ),
        name="layer",
    )(*operands)


def hand_over_kernel(*refs):
    n = len(refs) // 3
    sources, targets = refs[:n], refs[n : 2 * n]
    held, (fetched, written) = refs[2 * n : 3 * n], refs[3 * n :]

    def pieces(i):
        rows = sources[i].shape[0]
        parts = 4 if i < 3 else 1
        step = rows // parts
        return [(k, pl.ds(k * step, step)) for k in range(parts)]

    def fetch(i, k, rows):
        return pltpu.make_async_copy(sources[i].at[rows], held[i].at[rows], fetched.at[i, k])

    def write(i, k, rows):
        return pltpu.make_async_copy(held[i].at[rows], targets[i].at[rows], written.at[i, k])

    every = [(i, k, rows) for i in range(n) for k, rows in pieces(i)]
    for piece in every:
        fetch(*piece).start()
    for piece in every:
        fetch(*piece).wait()
        write(*piece).start()
    for piece in every:
        write(*piece).wait()


def hand_over(arrays):
    hbm = pl.BlockSpec(memory_space=pl.ANY)
    n = len(arrays)
    return pl.pallas_call(
        hand_over_kernel,
        out_shape=tuple(jax.ShapeDtypeStruct(a.shape, a.dtype) for a in arrays),
        in_specs=[hbm] * n,
        out_specs=(hbm,) * n,
        scratch_shapes=[pltpu.VMEM(a.shape, a.dtype) for a in arrays]
        + [pltpu.SemaphoreType.DMA((n, 4))] * 2,
        compiler_params=pltpu.CompilerParams(vmem_limit_bytes=62 * 1024 * 1024),
        name="hand_over",
    )(*arrays)


def shards(
    tokens,
    norm_gain,
    cotangent,
    routes,
    route_weight,
    gate_weight,
    up_weight,
    down_weight,
    scan_input,
    out_gate,
    step_size,
    decay_rate,
    write_keys,
    read_keys,
    start_state,
    out_proj,
):
    (
        gate_grad,
        up_grad,
        down_grad,
        residual_part,
        out_proj_grad,
        scan_grad,
        gate_out_grad,
        write_grad,
        read_grad,
    ) = hand_over(
        layer(
        tokens,
        cotangent,
        norm_gain[None, :],
        jnp.transpose(routes),
        jnp.transpose(route_weight),
        out_gate,
        scan_input,
        step_size,
        decay_rate,
        jnp.transpose(write_keys),
        jnp.transpose(read_keys),
        start_state[0],
        jnp.transpose(gate_weight[0]),
        jnp.transpose(up_weight[0]),
        down_weight[0],
        out_proj,
        )
    )
    return (
        residual_part,
        jnp.transpose(gate_grad)[None],
        jnp.transpose(up_grad)[None],
        down_grad[None],
        out_proj_grad,
        scan_grad,
        gate_out_grad,
        jnp.transpose(write_grad),
        jnp.transpose(read_grad),
    )


def solution(mesh):
    finer = Mesh(mesh.devices.reshape(8, 4, 2, mesh.shape["tp"]), ("sp_0", "sp_1", "sp_2", "tp"))
    in_specs = (
        P(SP, None),
        P(),
        P(SP, None),
        P(SP, None),
        P(SP, None),
        P(SP, None, "tp"),
        P(SP, None, "tp"),
        P(SP, "tp", None),
        P(SP, "tp"),
        P(SP, "tp"),
        P("tp", SP),
        P("tp"),
        P(SP, "tp"),
        P(SP, "tp"),
        P(SP, "tp", None, None),
        P(None, "tp"),
    )
    out_specs = (
        P(SP, "tp"),
        P(SP, None, "tp"),
        P(SP, None, "tp"),
        P(SP, "tp", None),
        P(SP, "tp"),
        P(SP, "tp"),
        P(SP, "tp"),
        P(SP, "tp"),
        P(SP, "tp"),
    )
    return jax.shard_map(
        shards, mesh=finer, in_specs=in_specs, out_specs=out_specs, check_vma=False
    )
```

time: 167 us -> 135 us (0.81)
  local copies, waits for them, and re-layouts: 16.8 us -> 0 us
  matrix products: 10.7 us -> 0 us
  other arithmetic: 4.07 us -> 0 us
    unnamed x37 -> x0, local copies, waits for them, and re-layouts: 10.8 us -> none
    dot_general x12 -> x0, matrix products: 10.7 us -> none  [the longest x1 2.09 us: shards(): jnp.dot(place_matrix, normed_q, preferred_element_type=jnp.float32)]
    pallas_call x0 -> x1, Pallas kernels: none -> 5.54 us  [hand_over(): pl.pallas_call(hand_over_kernel, out_shape=tuple((jax.ShapeDtypeStruct(a....]
    pallas_call x1, Pallas kernels: 134 us -> 129 us  [layer(): pl.pallas_call(layer_kernel, out_shape=(wide, wide, wide, shape((TOK, QUA...]
where the time goes in v3:
time: 135 us
  Pallas kernels  134 us (99%)
    pallas_call x1, Pallas kernels, layer(): pl.pallas_call(layer_kernel, out_shape=(wide, wide, wide, shape((TOK, QUA...  129 us
    pallas_call x1, Pallas kernels, hand_over(): pl.pallas_call(hand_over_kernel, out_shape=tuple((jax.ShapeDtypeStruct(a....  5.54 us

profile of v3, /device:TPU:1, one launch (start us, length us, event | category | flops | bytes accessed | tf_op | source)
XLA Modules:
  0.0 135.1 jit_solution(16760256562394631848)
XLA Ops:
  0.6 128.8 %layer.1 = (bf16[448,2048]{1,0:T(8,128)(2,1)}, bf16[448,2048]{1,0:T(8,128)(2,1)}, bf16[448,2048]{1,0:T(8,128)(2,1)}, bf16[128,512]{1,0:T(8,128)(2,1)}, f32[32,25...) custom-call(bf16[128,2048]{1,0:T(8,128)(2,1)} %tok_hbm.1, ...), custom_call_target="tpu_custom_call" | custom-call | tf_op jit(solution)/shard_map/layer/pallas_call | solution.py:880
  129.4 5.5 %hand_over.1 = (bf16[448,2048]{1,0:T(8,128)(2,1)}, bf16[448,2048]{1,0:T(8,128)(2,1)}, bf16[448,2048]{1,0:T(8,128)(2,1)}, bf16[128,512]{1,0:T(8,128)(2,1)}, f32[3...) custom-call(bf16[448,2048]{1,0:T(8,128)(2,1)} %get-tuple-element.27., ...), custom_call_target="tpu_custom_call" | custom-call | tf_op jit(solution)/shard_map/hand_over/pallas_call | solution.py:1022

commit v4 on v3

--- a/solution.py
+++ b/solution.py
@@ -45,7 +45,7 @@
 )
 RINGED = 5
 SLICE = TOK // NY
-PARTS = ((0, 256), (256, 128), (384, 128))
+PARTS = tuple((128 * i, 128) for i in range(4))
 PIECE = 16
 PACK = 128
 NT = (((1,), (1,)), ((), ()))
@@ -119,7 +119,7 @@
     later, res_box, prod, opg_box, pairs_w, scores, heads_u, heads_silu, heads_gate, heads_sg,
     heads_in, cols_t, reads, writes, res_out, opg_out, scan_out, gog_out, write_out, read_out,
     tok_ref, cotan_ref, gain_ref, routes_ref, route_weight_ref, og_ref, scan_ref, step_ref,
-    write_ref, read_ref, state_ref, tok_part, cotan_part, gain_part, li, lw, s1, r1, sy, ry, sm, rm, sgz, rgz, spm, rpm, sf, rf, sb, rb, ss, rs, sq, rq, sa, ra, sbb, rbb,
+    write_ref, read_ref, state_ref, tok_part, cotan_part, gain_part, credit, li, lw, s1, r1, sy, ry, sm, rm, sgz, rgz, spm, rpm, sf, rf, sb, rb, ss, rs, sq, rq, sa, ra, sbb, rbb,
     sc, rc, sr, rr, so, ro,
 ):
     z, x, c, y = position()
@@ -233,15 +233,20 @@
             staged(k, pl.ds(0, short)), block(k, 0, short, y), s1.at[k], r1.at[k], at(z, x, c, up)
         )
 
-    def relay(k, row, q, slot):
+    def relay(k, row, q):
         return remote(
-            block(k, row, HALF, q), block(k, row, HALF, q), sm.at[k, slot], rm.at[k, slot],
-            at(z, x, 1 - c, y),
+            block(k, row, HALF, q), block(k, row, HALF, q), sm.at[k], rm.at[k], at(z, x, 1 - c, y)
         )
+
+    def relayed(k):
+        array, _, width, _, _ = CHUNKS[k]
+        view = targets[array].at[pl.ds(0, ROWS if k < RINGED else HALF)]
+        view = view.at[:, pl.ds(0, 2 * width if k < RINGED else width)]
+        return remote(view, view, sm.at[k], rm.at[k], at(z, x, 1 - c, y))
 
     def along(k, row, rows, q, slot, target):
         return remote(
-            block(k, row, rows, q), block(k, row, rows, q), sy.at[k, slot], ry.at[k, slot],
+            block(k, row, rows, q), block(k, row, rows, q), sy.at[CHUNKS[k][0]], ry.at[k, slot],
             at(z, x, c, target),
         )
 
@@ -249,29 +254,27 @@
         whole(k).wait_recv()
         along(k, mine, HALF, y, 0, up).start()
         along(k, mine, HALF, y, 1, down).start()
-        relay(k, mine, y, 0).start()
+        relay(k, mine, y).start()
 
     def second(k):
         along(k, mine, HALF, down, 0, up).wait_recv()
         along(k, mine, part_rows, down, 2, up).start()
-        relay(k, mine, down, 1).start()
+        relay(k, mine, down).start()
         along(k, mine, HALF, up, 1, down).wait_recv()
         along(k, mine + part_rows, part_rows, up, 3, down).start()
-        relay(k, mine, up, 2).start()
+        relay(k, mine, up).start()
 
     def third(k):
         along(k, mine, part_rows, far, 2, up).wait_recv()
         along(k, mine + part_rows, part_rows, far, 3, down).wait_recv()
-        relay(k, mine, far, 3).start()
+        relay(k, mine, far).start()
 
     def straight(k):
         whole(k).wait_recv()
-        relay(k, mine, 0, 0).start()
+        relay(k, mine, 0).start()
 
     def gather(k):
-        for slot, q in enumerate((y, down, up, far)):
-            if slot == 0 or k < RINGED:
-                relay(k, other, q, slot).wait_recv()
+        relayed(k).wait_recv()
 
     def forward(array, columns, width, fresh):
         pairs = ((0, accg), (1, accu)) if array == 0 else ((2, acca),)
@@ -401,16 +404,20 @@
     third(0)
     third(1)
     first(3)
+    signal(credit, at(z, x, 1 - c, y))
     whole(4).wait_send()
+    pl.semaphore_wait(credit, 1)
     issue(5)
     loads[0].wait()
     loads[1].wait()
     second(2)
     first(4)
+    signal(credit, at(z, x, 1 - c, y))
     gather(0)
     gather(1)
     forward(0, ring_in, 256, True)
     whole(5).wait_send()
+    pl.semaphore_wait(credit, 1)
     issue(6)
     second(3)
     for d in range(1, NZ):
@@ -447,7 +454,7 @@
         times(HALF // 256, body)
 
     def to_mate(slot):
-        return remote(po.at[slot], mate.at[slot], spm.at[slot], rpm.at[slot], at(z, x, 1 - c, y))
+        return remote(po.at[slot], mate.at[slot], spm, rpm.at[slot], at(z, x, 1 - c, y))
 
     def fold(slot):
         to_mate(slot).wait_recv()
@@ -464,7 +471,7 @@
         return pl.ds(*PARTS[ch])
 
     def ring(src, dst, slot, ch, target):
-        return remote(src, dst, sf.at[slot, ch], rf.at[slot, ch], at(z, x, c, target))
+        return remote(src, dst, sf, rf.at[slot, ch], at(z, x, c, target))
 
     def f_up(ch):
         return ring(acc.at[0, lo, part(ch)], fwd.at[0, :, part(ch)], 0, ch, up)
@@ -511,7 +518,7 @@
             remote(
                 done.at[pl.ds(pl.multiple_of((pz * NX + px) * CAP, CAP), CAP), part(ch)],
                 back.at[own_rows, part(ch)],
-                sb.at[ch],
+                sb,
                 rb.at[ch],
                 at(pz, px, c, y),
             ).start()
@@ -522,7 +529,7 @@
 
     def all_back(ch):
         piece = (pl.ds(0, short), part(ch))
-        return remote(done.at[piece], back.at[piece], sb.at[ch], rb.at[ch], at(z, x, c, up))
+        return remote(done.at[piece], back.at[piece], sb, rb.at[ch], at(z, x, c, up))
 
     def weight_grads(start, stop):
         def step(i, carry):
@@ -575,27 +582,30 @@
         finish(ch)
         give_back(ch)
 
+    launch(1)
     turn(0)
-    launch(1)
+    launch(2)
     product(3, mine, pm)
     fold(3)
-    weight_grads(0, 2)
     turn(1)
-    launch(2)
-    weight_grads(2, 3)
+    launch(3)
+    weight_grads(0, 1)
     complete(0)
     turn(2)
-    weight_grads(3, 5)
+    weight_grads(1, 2)
     complete(1)
-    weight_grads(5, 6)
+    turn(3)
+    weight_grads(2, 4)
     complete(2)
+    weight_grads(4, 5)
+    complete(3)
 
     first_rows, second_rows = pl.ds(0, TOK // 2), pl.ds(TOK // 2, TOK // 2)
     everything = pl.ds(0, TOK)
 
     def share(q, piece, slot, target, ch):
         ref = share_buf.at[q, piece, part(ch)]
-        return remote(ref, ref, ss.at[slot, ch], rs.at[slot, ch], at(z, x, c, target))
+        return remote(ref, ref, ss, rs.at[slot, ch], at(z, x, c, target))
 
     def place(ch):
         all_back(ch).wait_recv()
@@ -609,49 +619,32 @@
         share(up, everything, 1, down, ch).wait_recv()
         share(up, second_rows, 3, down, ch).start()
 
+    def sent(view, sem):
+        remote(view, view, sem, sem, at(z, x, c, up)).wait_send()
+
     def sent_dispatch():
-        for k in range(RINGED):
-            along(k, mine, HALF, y, 0, up).wait_send()
-            along(k, mine, HALF, y, 1, down).wait_send()
-            along(k, mine, part_rows, down, 2, up).wait_send()
-            along(k, mine + part_rows, part_rows, up, 3, down).wait_send()
-            for slot, q in enumerate((y, down, up, far)):
-                relay(k, mine, q, slot).wait_send()
+        sent(rin.at[pl.ds(0, HALF), pl.ds(0, 3 * QUARTER)], sy.at[0])
+        sent(rcot.at[pl.ds(0, HALF), pl.ds(0, 3 * RING)], sy.at[1])
         whole(6).wait_send()
-        for k in range(RINGED, len(CHUNKS)):
-            relay(k, mine, 0, 0).wait_send()
+        for k in range(len(CHUNKS)):
+            relayed(k).wait_send()
 
     def sent_ring():
-        for slot in range(NY):
-            to_mate(slot).wait_send()
-        for ch in range(len(PARTS)):
-            for copy in (f_up, f_down, d_up, d_down, a_up, a_down, all_back):
-                copy(ch).wait_send()
-            share(y, everything, 0, up, ch).wait_send()
-            share(y, everything, 1, down, ch).wait_send()
-            share(down, first_rows, 2, up, ch).wait_send()
-            share(up, second_rows, 3, down, ch).wait_send()
+        sent(po, spm)
+        sent(acc.at[pl.ds(0, 3)], sf)
+        sent(done.at[pl.ds(0, short)], sb)
+        sent(share_buf.at[pl.ds(0, 3)], ss)
 
     def sent_carry():
-        for d in range(1, NW):
-            p, device = plane_mate(d)
-            remote(msg.at[p], box_a.at[w], sa.at[d], ra.at[d], device).wait_send()
-            remote(plane, box_b.at[z], sbb.at[d], rbb.at[d], line_peer(d)[1]).wait_send()
-            send_res(d, z).wait_send()
-        ring_res(y, every, 0, up).wait_send()
-        ring_res(y, every, 1, down).wait_send()
+        sent(msg.at[pl.ds(0, NW - 1)], sa)
+        sent(box_b.at[pl.ds(0, NZ - 1)], sbb)
+        sent(res_box.at[0, pl.ds(0, (NZ - 1) * SLICE)], sr)
 
     place(0)
-    weight_grads(6, 8)
-    outs = [
-        pltpu.make_async_copy(wg.at[i], hbm, lw.at[4 + i])
-        for i, hbm in enumerate((gg_hbm, ug_hbm, dg_hbm))
-    ]
-    for out in outs:
-        out.start()
+    outs = []
 
     def put(ref, hbm):
-        copy = pltpu.make_async_copy(ref, hbm, lw.at[4 + len(outs)])
+        copy = pltpu.make_async_copy(ref, hbm, lw.at[7 + len(outs)])
         copy.start()
         outs.append(copy)
 
@@ -659,7 +652,9 @@
     pass_shares(0)
     place(2)
     pass_shares(1)
+    place(3)
     pass_shares(2)
+    pass_shares(3)
     dotted = jnp.zeros((TOK, 1), F32)
 
     def dotted_with(q):
@@ -698,7 +693,7 @@
     def send_res(d, source):
         p, device = line_peer(d)
         return remote(
-            res.at[slice_rows, pl.ds(mult(p, CH), CH)], boxed(source), sr.at[d], rr.at[d], device
+            res.at[slice_rows, pl.ds(mult(p, CH), CH)], boxed(source), sr, rr, device
         )
 
     for d in range(1, NZ):
@@ -721,7 +716,7 @@
             )
     for d in range(1, NW):
         p, device = plane_mate(d)
-        remote(msg.at[p], box_a.at[w], sa.at[d], ra.at[d], device).start()
+        remote(msg.at[p], box_a.at[w], sa, ra, device).start()
     box_a[w] = msg[w]
     read_grads, write_grads = [], []
 
@@ -738,14 +733,11 @@
         write_grads.append(dot(pair_terms, read, TN, HIGHEST))
 
     head_back(0)
+    weight_grads(5, 6)
     head_back(1)
 
-    def source_of(d):
-        return lax.rem(w + NW - d, NW)
-
-    for d in range(1, NW):
-        p, device = plane_mate(d)
-        remote(msg.at[p], box_a.at[source_of(d)], sa.at[d], ra.at[d], device).wait_recv()
+    seven_a = box_a.at[pl.ds(0, NW - 1)]
+    remote(seven_a, seven_a, sa, ra, at(z, x, c, up)).wait_recv()
     data, scale = pl.ds(0, PIECE), pl.ds(PIECE, 8)
 
     def pair(ref, i):
@@ -767,13 +759,13 @@
     box_b[z, data, :] = total
     box_b[z, scale, :] = decay[0:8, :]
     for d in range(1, NZ):
-        remote(plane, box_b.at[z], sbb.at[d], rbb.at[d], line_peer(d)[1]).start()
-    for d in range(1, NZ):
-        send_res(d, lax.rem(z + NZ - d, NZ)).wait_recv()
+        remote(plane, box_b.at[z], sbb, rbb, line_peer(d)[1]).start()
+    seven_res = res_box.at[y, pl.ds(0, (NZ - 1) * SLICE)]
+    remote(seven_res, seven_res, sr, rr, at(z, x, c, up)).wait_recv()
 
     def ring_res(q, rows, slot, target):
         ref = res_box.at[q, rows, :]
-        return remote(ref, ref, sq.at[slot], rq.at[slot], at(z, x, c, target))
+        return remote(ref, ref, sq, rq.at[slot], at(z, x, c, target))
 
     every, early, late = (
         pl.ds(0, NZ * SLICE),
@@ -783,9 +775,15 @@
     ring_res(y, every, 0, up).start()
     ring_res(y, every, 1, down).start()
     head_back(2)
-    for d in range(1, NZ):
-        source = lax.rem(z + NZ - d, NZ)
-        remote(plane, box_b.at[source], sbb.at[d], rbb.at[d], line_peer(d)[1]).wait_recv()
+    weight_grads(6, 8)
+    wide_outs = [
+        pltpu.make_async_copy(wg.at[i], hbm, lw.at[4 + i])
+        for i, hbm in enumerate((gg_hbm, ug_hbm, dg_hbm))
+    ]
+    for out in wide_outs:
+        out.start()
+    seven_b = box_b.at[pl.ds(0, NZ - 1)]
+    remote(seven_b, seven_b, sbb, rbb, at(z, x, c, up)).wait_recv()
     beyond = jnp.zeros((PIECE, PACK), F32)
     for k in reversed(range(1, NZ)):
         value, factor = pair(box_b, k)
@@ -798,7 +796,7 @@
 
     for d in range(1, NW):
         p, device = plane_mate(d)
-        remote(fan.at[p], slot_of(w), sc.at[d], rc.at[d], device).start()
+        remote(fan.at[p], slot_of(w), sc, rc, device).start()
     later[w] = fan[w]
     head_back(3)
     put(gog_out, gog_hbm)
@@ -809,9 +807,8 @@
     ring_res(up, late, 3, down).start()
     seven = gz.at[pl.ds(0, (NZ - 1) * TOK), :]
     remote(seven, seven, sgz, rgz, at(z, x, c, up)).wait()
-    for d in range(1, NW):
-        p, device = plane_mate(d)
-        remote(fan.at[p], slot_of(source_of(d)), sc.at[d], rc.at[d], device).wait_recv()
+    seven_c = later.at[pl.ds(0, NW - 1)]
+    remote(seven_c, seven_c, sc, rc, at(z, x, c, up)).wait_recv()
 
     def head_end(h):
         lanes = slice(h * HD, (h + 1) * HD)
@@ -839,29 +836,25 @@
     prod[...] = value.reshape(prod.shape).astype(BF16)
     for d in range(1, NW):
         p, device = plane_mate(d)
-        remote(prod.at[p], opg_box.at[w], so.at[d], ro.at[d], device).start()
+        remote(prod.at[p], opg_box.at[w], so, ro, device).start()
     opg_box[w] = prod[w]
     write_out[...] = jnp.transpose(sum(write_grads[1:], write_grads[0])).astype(BF16)
     read_out[...] = jnp.transpose(sum(read_grads[1:], read_grads[0])).astype(BF16)
     put(write_out, write_hbm)
     put(read_out, read_hbm)
     sent_carry()
-    for d in range(1, NW):
-        p, device = plane_mate(d)
-        remote(prod.at[p], opg_box.at[source_of(d)], so.at[d], ro.at[d], device).wait_recv()
+    seven_o = opg_box.at[pl.ds(0, NW - 1)]
+    remote(seven_o, seven_o, so, ro, at(z, x, c, up)).wait_recv()
     opg = opg_box[0].astype(F32)
     for k in range(1, NW):
         opg = opg + opg_box[k].astype(F32)
     opg_out[...] = opg
     put(opg_out, opg_hbm)
 
-    for d in range(1, NW):
-        p, device = plane_mate(d)
-        remote(fan.at[p], slot_of(w), sc.at[d], rc.at[d], device).wait_send()
-        remote(prod.at[p], opg_box.at[w], so.at[d], ro.at[d], device).wait_send()
-    ring_res(down, early, 2, up).wait_send()
-    ring_res(up, late, 3, down).wait_send()
-    for out in outs:
+    sent(fan.at[pl.ds(0, NW - 1)], sc)
+    sent(prod.at[pl.ds(0, NW - 1)], so)
+    sent(res_box.at[pl.ds(0, 3)], sq)
+    for out in wide_outs + outs:
         out.wait()
 
 
@@ -960,28 +953,29 @@
             held(TOK, QUARTER),
             held(TOK, RING),
             held(1, QUARTER, dtype=F32),
+            pltpu.SemaphoreType.REGULAR,
             dma((14,)),
             dma((13,)),
             dma((n,)),
             dma((n,)),
-            dma((n, 4)),
-            dma((n, 4)),
-            dma((n, 4)),
-            dma((n, 4)),
+            dma((2,)),
+            dma((RINGED, 4)),
+            dma((n,)),
+            dma((n,)),
+            dma,
             dma,
             dma,
             dma((NY,)),
-            dma((NY,)),
+            dma,
             dma((6, len(PARTS))),
-            dma((6, len(PARTS))),
+            dma,
             dma((len(PARTS),)),
-            dma((len(PARTS),)),
+            dma,
             dma((4, len(PARTS))),
-            dma((4, len(PARTS))),
-            dma((4,)),
+            dma,
             dma((4,)),
         ]
-        + [dma((8,))] * 10,
+        + [dma] * 10,
         compiler_params=pltpu.CompilerParams(
             collective_id=0, has_side_effects=True, vmem_limit_bytes=62 * 1024 * 1024
         ),

time: 135 us -> 131 us (0.970)
  Pallas kernels: 134 us -> 131 us
    pallas_call x1, Pallas kernels: 129 us -> 125 us  [layer(): pl.pallas_call(layer_kernel, out_shape=(wide, wide, wide, shape((TOK, QUA...]
where the time goes in v4:
time: 131 us
  Pallas kernels  131 us (100%)
    pallas_call x1, Pallas kernels, layer(): pl.pallas_call(layer_kernel, out_shape=(wide, wide, wide, shape((TOK, QUA...  125 us
    pallas_call x1, Pallas kernels, hand_over(): pl.pallas_call(hand_over_kernel, out_shape=tuple((jax.ShapeDtypeStruct(a....  5.54 us

profile of v4, /device:TPU:1, one launch (start us, length us, event | category | flops | bytes accessed | tf_op | source)
XLA Modules:
  0.0 131.3 jit_solution(8687652382406376981)
XLA Ops:
  0.6 125.0 %layer.1 = (bf16[448,2048]{1,0:T(8,128)(2,1)}, bf16[448,2048]{1,0:T(8,128)(2,1)}, bf16[448,2048]{1,0:T(8,128)(2,1)}, bf16[128,512]{1,0:T(8,128)(2,1)}, f32[32,25...) custom-call(bf16[128,2048]{1,0:T(8,128)(2,1)} %tok_hbm.1, ...), custom_call_target="tpu_custom_call" | custom-call | tf_op jit(solution)/shard_map/layer/pallas_call | solution.py:873
  125.6 5.5 %hand_over.1 = (bf16[448,2048]{1,0:T(8,128)(2,1)}, bf16[448,2048]{1,0:T(8,128)(2,1)}, bf16[448,2048]{1,0:T(8,128)(2,1)}, bf16[128,512]{1,0:T(8,128)(2,1)}, f32[3...) custom-call(bf16[448,2048]{1,0:T(8,128)(2,1)} %get-tuple-element.27., ...), custom_call_target="tpu_custom_call" | custom-call | tf_op jit(solution)/shard_map/hand_over/pallas_call | solution.py:1016

commit v5 on v4

--- a/solution.py
+++ b/solution.py
@@ -91,6 +91,7 @@
     for d in range(NX):
         signal(barrier, at(z, lax.rem(x + d, NX), 1 - c, y))
     signal(barrier, at(z, x, c, lax.rem(y + 1, NY)))
+    signal(barrier, at(z, x, c, lax.rem(y + 2, NY)))
     signal(barrier, at(z, x, c, lax.rem(y + 3, NY)))
 
 
@@ -199,7 +200,7 @@
     rin[kept_rows, own_cols] = sin[own_rows, :]
     rcot[kept_rows, ring_cols] = scot[own_rows, 0:RING]
     rcot[kept_rows, 0:DIRECT] = scot[own_rows, RING:]
-    pl.semaphore_wait(barrier, CHIPS - 1 + NX + 2)
+    pl.semaphore_wait(barrier, CHIPS - 1 + NX + 3)
 
     def block(k, row, rows, q):
         array, _, width, base, stride = CHUNKS[k]
@@ -600,7 +601,6 @@
     weight_grads(4, 5)
     complete(3)
 
-    first_rows, second_rows = pl.ds(0, TOK // 2), pl.ds(TOK // 2, TOK // 2)
     everything = pl.ds(0, TOK)
 
     def share(q, piece, slot, target, ch):
@@ -612,12 +612,7 @@
         share_buf[y, :, part(ch)] = dot(slots[...], back[:, part(ch)], TN).astype(BF16)
         share(y, everything, 0, up, ch).start()
         share(y, everything, 1, down, ch).start()
-
-    def pass_shares(ch):
-        share(down, everything, 0, up, ch).wait_recv()
-        share(down, first_rows, 2, up, ch).start()
-        share(up, everything, 1, down, ch).wait_recv()
-        share(up, second_rows, 3, down, ch).start()
+        share(y, everything, 2, far, ch).start()
 
     def sent(view, sem):
         remote(view, view, sem, sem, at(z, x, c, up)).wait_send()
@@ -648,13 +643,11 @@
         copy.start()
         outs.append(copy)
 
-    place(1)
-    pass_shares(0)
-    place(2)
-    pass_shares(1)
-    place(3)
-    pass_shares(2)
-    pass_shares(3)
+    for ch in range(1, len(PARTS)):
+        place(ch)
+    for ch in range(len(PARTS)):
+        share(down, everything, 0, up, ch).wait_recv()
+        share(up, everything, 1, down, ch).wait_recv()
     dotted = jnp.zeros((TOK, 1), F32)
 
     def dotted_with(q):
@@ -666,8 +659,7 @@
     sent_dispatch()
     dotted += dotted_with(y) + dotted_with(down) + dotted_with(up)
     for ch in range(len(PARTS)):
-        share(far, first_rows, 2, up, ch).wait_recv()
-        share(far, second_rows, 3, down, ch).wait_recv()
+        share(far, everything, 2, far, ch).wait_recv()
 
     dotted += dotted_with(far)
     coef = inv * inv * inv * dotted / D
@@ -971,7 +963,7 @@
             dma,
             dma((len(PARTS),)),
             dma,
-            dma((4, len(PARTS))),
+            dma((3, len(PARTS))),
             dma,
             dma((4,)),
         ]

time: 131 us -> 129 us (0.985)
  Pallas kernels: 131 us -> 128 us
    pallas_call x1, Pallas kernels: 125 us -> 123 us  [layer(): pl.pallas_call(layer_kernel, out_shape=(wide, wide, wide, shape((TOK, QUA...]
where the time goes in v5:
time: 129 us
  Pallas kernels  128 us (99%)
    pallas_call x1, Pallas kernels, layer(): pl.pallas_call(layer_kernel, out_shape=(wide, wide, wide, shape((TOK, QUA...  123 us
    pallas_call x1, Pallas kernels, hand_over(): pl.pallas_call(hand_over_kernel, out_shape=tuple((jax.ShapeDtypeStruct(a....  5.54 us

profile of v5, /device:TPU:1, one launch (start us, length us, event | category | flops | bytes accessed | tf_op | source)
XLA Modules:
  0.0 129.0 jit_solution(12675655365406943013)
XLA Ops:
  0.6 122.7 %layer.1 = (bf16[448,2048]{1,0:T(8,128)(2,1)}, bf16[448,2048]{1,0:T(8,128)(2,1)}, bf16[448,2048]{1,0:T(8,128)(2,1)}, bf16[128,512]{1,0:T(8,128)(2,1)}, f32[32,25...) custom-call(bf16[128,2048]{1,0:T(8,128)(2,1)} %tok_hbm.1, ...), custom_call_target="tpu_custom_call" | custom-call | tf_op jit(solution)/shard_map/layer/pallas_call | solution.py:865
  123.3 5.5 %hand_over.1 = (bf16[448,2048]{1,0:T(8,128)(2,1)}, bf16[448,2048]{1,0:T(8,128)(2,1)}, bf16[448,2048]{1,0:T(8,128)(2,1)}, bf16[128,512]{1,0:T(8,128)(2,1)}, f32[3...) custom-call(bf16[448,2048]{1,0:T(8,128)(2,1)} %get-tuple-element.27., ...), custom_call_target="tpu_custom_call" | custom-call | tf_op jit(solution)/shard_map/hand_over/pallas_call | solution.py:1008
